TPU v7x, 32 devices: a whole 2x2x4 slice. The times are simulated.
32 devices in a mesh: sp: 8 (over z, x), tp: 4 (over y, core).
Axes of the slice: x: 2, y: 2, z: 4, core: 2. Of those that a mesh axis runs over, the one named last changes fastest.
Arguments:
- layer_input: bfloat16 [1024, 2048], P('sp', 'tp'), may hold values from -6 to 6
- cotangent: bfloat16 [1024, 2048], P('sp', 'tp'), may hold values from -6 to 6
- routes: int32 [1024, 2], P('sp'), may hold values from 0 to 7, all different within a row; in each aligned block of 128 rows (0 to 127, 128 to 255, ...) at most 48 rows name the same one
- route_weight: float32 [1024, 2], P('sp'), may hold values from 0.1 to 0.6
- gate_weight: bfloat16 [8, 2048, 1024], P('sp', None, 'tp'), may hold values from -0.125 to 0.125
- up_weight: bfloat16 [8, 2048, 1024], P('sp', None, 'tp'), may hold values from -0.125 to 0.125
- down_weight: bfloat16 [8, 1024, 2048], P('sp', 'tp'), may hold values from -0.1875 to 0.1875
- heads_value: bfloat16 [1024, 2048], P('sp', 'tp'), may hold values from -6 to 6
- output_gate: bfloat16 [1024, 2048], P('sp', 'tp'), may hold values from -8 to 8
- mixer_saved: bfloat16 [1024, 2048], P('sp', 'tp'), may hold values from -6 to 6
- proj_weight: bfloat16 [2048, 2048], P(None, 'tp'), may hold values from -0.125 to 0.125
- state_write: bfloat16 [1024, 512], P('sp', 'tp'), may hold values from -0.5 to 0.5
- state_read: bfloat16 [1024, 512], P('sp', 'tp'), may hold values from -0.5 to 0.5
- decay_rate: float32 [1024, 32], P('sp', 'tp'), may hold values from 0 to 1.1, as said below
Outputs:
- gate_grad: bfloat16 [8, 2048, 1024], P('sp', None, 'tp')
- up_grad: bfloat16 [8, 2048, 1024], P('sp', None, 'tp')
- down_grad: bfloat16 [8, 1024, 2048], P('sp', 'tp')
- proj_grad: float32 [2048, 2048], P('sp', 'tp')
- value_grad: bfloat16 [1024, 2048], P('sp', 'tp')
- write_gradient: bfloat16 [1024, 512], P('sp', 'tp')
- read_gradient: bfloat16 [1024, 512], P('sp', 'tp')
- outgate_grad: bfloat16 [1024, 2048], P('sp', 'tp')
Inputs may be any that keep to these rules, and one draw needn't show every extreme that they name: `routes`: each row names 2 different experts; within the rows of one aligned block of 128 tokens no expert is named by more than 48 rows, a bound that some block reaches. `decay_rate`: positive log-decays.
All inputs are finite; a program needn't handle non-finite values.
Results may differ from a plain program's by a relative error of at most 0.017.
Values may be sent and summed in bfloat16 or wider, within the bound.
A program may use at most 128 MiB of HBM per device.

v0:
```python
import functools

import jax
import jax.numpy as jnp
from jax import lax
from jax.experimental import pallas as pl
from jax.experimental.pallas import tpu as pltpu
from jax.sharding import PartitionSpec as P

HEAD_DIM = 64
STATE = 128
MESH = pl.DeviceIdType.MESH
LAST = (((1,), (1,)), ((), ()))
FIRST = (((0,), (0,)), ((), ()))
F32 = jnp.float32
BF16 = jnp.bfloat16
VMEM = pltpu.VMEM
DMA = pltpu.SemaphoreType.DMA


def silu_parts(value):
    sigma = jax.nn.sigmoid(value)
    return (value * sigma, sigma * (1.0 + value * (1.0 - sigma)))


class Place:
    def __init__(self, n, t):
        self.n, self.t = n, t
        self.sp = lax.axis_index("sp")
        self.tp = lax.axis_index("tp")
        self.across = lax.rem(self.tp + t // 2, t)
        self.beside = self.tp + 1 - 2 * lax.rem(self.tp, 2)
        self.cross = lax.rem(self.beside + t // 2, t)

    def to(self, src, dst, send, recv, sp=None, tp=None):
        return pltpu.make_async_remote_copy(
            src_ref=src,
            dst_ref=dst,
            send_sem=send,
            recv_sem=recv,
            device_id=(self.sp if sp is None else sp, self.tp if tp is None else tp),
            device_id_type=MESH,
        )

    def greet(self, sp_too=True):
        barrier = pltpu.get_barrier_semaphore()
        for tp in (self.across, self.beside):
            pl.semaphore_signal(barrier, inc=1, device_id=(self.sp, tp), device_id_type=MESH)
        count = 2
        if sp_too:
            for o in range(1, self.n):
                pl.semaphore_signal(
                    barrier,
                    inc=1,
                    device_id=(lax.rem(self.sp + o, self.n), self.tp),
                    device_id_type=MESH,
                )
            count += self.n - 1
        pl.semaphore_wait(barrier, count)


def loop(lo, hi, body):
    def step(i, carry):
        body(i)
        return carry

    lax.fori_loop(lo, hi, step, 0)


def dispatch_kernel(
    n, t, x_ref, c_ref, a_ref, xo, co, ao, s_a2a, r_a2a, s_sh, r_sh, s_d, r_d, own_sem
):
    at = Place(n, t)
    d = x_ref.shape[2]
    col = lambda tp: pl.ds(pl.multiple_of(tp * d, d), d)
    sides = ((x_ref, xo), (c_ref, co))
    at.greet()

    def spread(k, o):
        src, dst = sides[k]
        peer = lax.rem(at.sp + o, n)
        return at.to(
            src.at[peer], dst.at[at.sp, :, col(at.tp)], s_a2a.at[k, o], r_a2a.at[k, o], sp=peer
        )

    def decay(o):
        peer = lax.rem(at.sp + o, n)
        return at.to(a_ref, ao.at[at.sp], s_d.at[o], r_d.at[o], sp=peer)

    def share(k, o, j):
        here = sides[k][1].at[lax.rem(at.sp + n - o, n), :, col(at.across if j == 2 else at.tp)]
        return at.to(
            here, here, s_sh.at[k, j, o], r_sh.at[k, j, o], tp=at.across if j == 0 else at.beside
        )

    owns = [
        pltpu.make_async_copy(
            src.at[at.sp], dst.at[at.sp, :, col(at.tp)], own_sem.at[k]
        )
        for k, (src, dst) in enumerate(sides)
    ]
    owns.append(pltpu.make_async_copy(a_ref, ao.at[at.sp], own_sem.at[2]))
    for own in owns:
        own.start()
    for k in (0, 1):
        loop(1, n, lambda o: spread(k, o).start())
    loop(1, n, lambda o: decay(o).start())
    for k in (0, 1):
        owns[k].wait()
        share(k, 0, 0).start()
        share(k, 0, 1).start()
    owns[2].wait()
    for k in (0, 1):

        def arrive(o):
            spread(k, o).wait_recv()
            share(k, o, 0).start()
            share(k, o, 1).start()
            share(k, o - 1, 0).wait_recv()
            share(k, o - 1, 2).start()

        loop(1, n, arrive)
        share(k, n - 1, 0).wait_recv()
        share(k, n - 1, 2).start()

    def finish(o):
        for k in (0, 1):
            share(k, o, 1).wait_recv()
            share(k, o, 2).wait_recv()
            for j in (0, 1, 2):
                share(k, o, j).wait_send()

    loop(0, n, finish)

    def finish_spread(o):
        for k in (0, 1):
            spread(k, o).wait_send()
        decay(o).wait()

    loop(1, n, finish_spread)


def combine_kernel(n, t, p_ref, out, pair, summed, other, final, s_p, r_p, s_y, r_y, s_a, r_a, own):
    at = Place(n, t)
    d = out.shape[2]
    col = lambda tp: pl.ds(pl.multiple_of(tp * d, d), d)
    at.greet()
    halves = [
        at.to(p_ref.at[:, :, col(c)], pair.at[k], s_p.at[k], r_p.at[k], tp=at.beside)
        for k, c in enumerate((at.cross, at.beside))
    ]
    for half in halves:
        half.start()

    def over(o):
        b = lax.rem(at.sp + o, n)
        return at.to(summed.at[b], other.at[b], s_y.at[o], r_y.at[o], tp=at.across)

    def back(o):
        b = lax.rem(at.sp + o, n)
        return at.to(final.at[b], out.at[at.sp], s_a.at[o], r_a.at[o], sp=b)

    halves[0].wait_recv()

    def add_pair(o):
        b = lax.rem(at.sp + o, n)
        summed[b] = (
            p_ref[b, :, col(at.across)].astype(F32) + pair[0, b].astype(F32)
        ).astype(BF16)
        over(o).start()

    def turn(i):
        o = i + 1
        add_pair(lax.rem(o, n))

    loop(0, n, turn)
    halves[1].wait_recv()

    def total(o):
        b = lax.rem(at.sp + o, n)
        over(o).wait_recv()
        final[b] = (
            p_ref[b, :, col(at.tp)].astype(F32) + pair[1, b].astype(F32) + other[b].astype(F32)
        ).astype(BF16)

    def total_and_send(o):
        total(o)
        back(o).start()

    loop(1, n, total_and_send)
    total(0)
    mine = pltpu.make_async_copy(final.at[at.sp], out.at[at.sp], own.at[0])
    mine.start()
    mine.wait()
    for half in halves:
        half.wait_send()
    loop(0, n, lambda o: over(o).wait_send())
    loop(1, n, lambda o: back(o).wait())


def rows_kernel(n, t, g_ref, out, s_sh, r_sh, own):
    at = Place(n, t)
    d = g_ref.shape[1]
    col = lambda tp: pl.ds(pl.multiple_of(tp * d, d), d)
    at.greet(sp_too=False)
    mine = pltpu.make_async_copy(g_ref, out.at[:, col(at.tp)], own.at[0])
    mine.start()
    first = at.to(g_ref, out.at[:, col(at.tp)], s_sh.at[0], r_sh.at[0], tp=at.across)
    side = at.to(g_ref, out.at[:, col(at.tp)], s_sh.at[1], r_sh.at[1], tp=at.beside)
    first.start()
    side.start()
    here = out.at[:, col(at.across)]
    onward = at.to(here, here, s_sh.at[2], r_sh.at[2], tp=at.beside)
    first.wait_recv()
    onward.start()
    mine.wait()
    side.wait()
    first.wait_send()
    onward.wait()


def late_kernel(n, t, *refs):
    wide = (1, 2)
    count = 5
    ins, g_ref, outs, gall = refs[:count], refs[count], refs[6 : 6 + count], refs[11]
    s_g, r_g, s_sh, r_sh, s_x, r_x, s_l, r_l, s_t, r_t, own = refs[12:]
    at = Place(n, t)
    q = g_ref.shape[1] // t
    row = lambda tp: pl.ds(pl.multiple_of(tp * q, q), q)
    length = n // 2
    z = at.sp // 2
    bit = lax.rem(at.sp, 2)
    twin = z * 2 + 1 - bit
    at.greet()
    keeps = [
        pltpu.make_async_copy(ins[a], outs[a].at[at.sp], own.at[a]) for a in range(count)
    ]
    keeps.append(pltpu.make_async_copy(g_ref.at[at.sp], gall.at[at.sp], own.at[count]))
    for keep in keeps:
        keep.start()
    pairs = [
        at.to(ins[a], outs[a].at[at.sp], s_x.at[a], r_x.at[a], sp=twin) for a in range(count)
    ]

    def spread(o):
        peer = lax.rem(at.sp + o, n)
        return at.to(
            g_ref.at[peer, row(at.tp), :],
            gall.at[at.sp, row(at.tp), :],
            s_g.at[o],
            r_g.at[o],
            sp=peer,
        )

    def share(o, j):
        here = gall.at[lax.rem(at.sp + n - o, n), row(at.across if j == 2 else at.tp), :]
        return at.to(
            here, here, s_sh.at[j, o], r_sh.at[j, o], tp=at.across if j == 0 else at.beside
        )

    def block_of(up, k, same):
        return (z - k if up else z + k) * 2 + (bit if same else 1 - bit)

    def hop(a, up, k, same):
        here = outs[a].at[block_of(up, k, same)]
        i, j = (0 if up else 1), (0 if same else 1)
        peer = z + 1 if up else z - 1
        return at.to(here, here, s_l.at[a, i, j, k], r_l.at[a, i, j, k], sp=peer * 2 + bit)

    def came(a, up, k, same):
        here = outs[a].at[block_of(up, k, same)]
        i, j = (0 if up else 1), (0 if same else 1)
        return at.to(here, here, s_l.at[a, i, j, k], r_l.at[a, i, j, k - 1], sp=twin)

    def side(a, up, k):
        here = outs[a].at[block_of(up, k, True)]
        i = 0 if up else 1
        return at.to(here, here, s_t.at[a, i, k], r_t.at[a, i, k], sp=twin)

    def sides_of(a):
        return (True,) if a in wide else (True, False)

    for a in range(count):
        if a not in wide:
            pairs[a].start()
    loop(1, n, lambda o: spread(o).start())
    order = wide + tuple(a for a in range(count) if a not in wide)

    def begin(a, same):
        @pl.when(z < length - 1)
        def _():
            hop(a, True, 0, same).start()

        @pl.when(z > 0)
        def _():
            hop(a, False, 0, same).start()

    for a in order:
        keeps[a].wait()
        begin(a, True)
    for a in order:
        if a in wide:
            pairs[a].start()
        else:
            pairs[a].wait_recv()
            begin(a, False)

    def arrive(o):
        spread(o).wait_recv()
        share(o, 0).start()
        share(o, 1).start()

    def advance(k):
        for a in order:
            for same in sides_of(a):

                @pl.when(z - k >= 0)
                def _():
                    came(a, True, k, same).wait_recv()

                    @pl.when(z < length - 1)
                    def _():
                        hop(a, True, k, same).start()

                    if a in wide:
                        side(a, True, k).start()

                @pl.when(z + k < length)
                def _():
                    came(a, False, k, same).wait_recv()

                    @pl.when(z > 0)
                    def _():
                        hop(a, False, k, same).start()

                    if a in wide:
                        side(a, False, k).start()

    loop(1, length, advance)
    keeps[count].wait()
    loop(1, n, arrive)

    def onward(o):
        share(o, 0).wait_recv()
        share(o, 2).start()

    loop(1, n, onward)

    def finish(o):
        share(o, 1).wait_recv()
        share(o, 2).wait_recv()
        for j in (0, 1, 2):
            share(o, j).wait_send()
        spread(o).wait_send()

    loop(1, n, finish)

    def drain(k):
        for a in order:
            for same in sides_of(a):

                @pl.when(jnp.logical_and(z - k >= 0, z < length - 1))
                def _():
                    hop(a, True, k, same).wait_send()

                @pl.when(jnp.logical_and(z + k < length, z > 0))
                def _():
                    hop(a, False, k, same).wait_send()

    loop(0, length, drain)

    def settle(k):
        for a in wide:

            @pl.when(z - k >= 0)
            def _():
                side(a, True, k).wait()

            @pl.when(z + k < length)
            def _():
                side(a, False, k).wait()

    loop(1, length, settle)
    for a in range(count):
        if a in wide:
            pairs[a].wait_recv()
        pairs[a].wait_send()


def mixer_kernel(chunk, dall, vall, rall, wall, arow, acol, dl, vl, rl, wl, vg, wg, rg):
    heads = acol.shape[1]
    per = heads * STATE // wl.shape[1]
    total = dall.shape[0]
    vg_sum = [jnp.zeros((dl.shape[0], HEAD_DIM), F32) for _ in range(heads)]
    wg_sum = [jnp.zeros((dl.shape[0], STATE), F32) for _ in range(heads // per)]
    rg_sum = [jnp.zeros((dl.shape[0], STATE), F32) for _ in range(heads // per)]

    def dot_last(a, b):
        return lax.dot_general(a, b, LAST, preferred_element_type=F32)

    def step(i, carry):
        vg_sum, wg_sum, rg_sum = carry
        vg_sum, wg_sum, rg_sum = list(vg_sum), list(wg_sum), list(rg_sum)
        rows = pl.ds(pl.multiple_of(i * chunk, chunk), chunk)
        for g in range(heads // per):
            wide = slice(g * STATE, (g + 1) * STATE)
            read, write = rall[rows, wide], wall[rows, wide]
            common = dot_last(wl[:, wide], read)
            q1 = jnp.zeros((dl.shape[0], chunk), F32)
            q2 = jnp.zeros((dl.shape[0], chunk), F32)
            for h in range(g * per, (g + 1) * per):
                cols = slice(h * HEAD_DIM, (h + 1) * HEAD_DIM)
                delta, value = dall[rows, cols], vall[rows, cols]
                fade = jnp.exp(-jnp.abs(acol[:, h : h + 1] - arow[h : h + 1, rows]))
                vg_sum[h] += jnp.dot(
                    (fade * common).astype(BF16), delta, preferred_element_type=F32
                )
                q1 += fade * dot_last(vl[:, cols], delta)
                q2 += fade * dot_last(dl[:, cols], value)
            wg_sum[g] += jnp.dot(q1.astype(BF16), read, preferred_element_type=F32)
            rg_sum[g] += jnp.dot(q2.astype(BF16), write, preferred_element_type=F32)
        return tuple(vg_sum), tuple(wg_sum), tuple(rg_sum)

    vg_sum, wg_sum, rg_sum = lax.fori_loop(
        0, total // chunk, step, (tuple(vg_sum), tuple(wg_sum), tuple(rg_sum))
    )
    for h in range(heads):
        vg[:, h * HEAD_DIM : (h + 1) * HEAD_DIM] = vg_sum[h].astype(BF16)
    for g in range(heads // per):
        wg[:, g * STATE : (g + 1) * STATE] = wg_sum[g].astype(BF16)
        rg[:, g * STATE : (g + 1) * STATE] = rg_sum[g].astype(BF16)


def call(kernel, ident, ins, outs, scratch, operands, name):
    vm = pl.BlockSpec(memory_space=pltpu.VMEM)
    return pl.pallas_call(
        kernel,
        out_shape=outs,
        in_specs=[vm] * ins,
        out_specs=jax.tree.map(lambda _: vm, outs),
        scratch_shapes=scratch,
        compiler_params=pltpu.CompilerParams(
            collective_id=ident,
            has_side_effects=ident is not None,
            vmem_limit_bytes=56 * 1024 * 1024,
        ),
        cost_estimate=pl.CostEstimate(
            flops=4_000_000_000, bytes_accessed=8_000_000, transcendentals=0
        ),
        name=name,
    )(*operands)


def on_device(
    layer_input,
    cotangent,
    routes,
    route_weight,
    gate_weight,
    up_weight,
    down_weight,
    heads_value,
    output_gate,
    mixer_saved,
    proj_weight,
    state_write,
    state_read,
    decay_rate,
):
    n = lax.axis_size("sp")
    t = lax.axis_size("tp")
    me = lax.axis_index("sp")
    tokens, d = layer_input.shape
    top = routes.shape[1]
    capacity = max(2, 3 * tokens * top // (2 * n))
    slots_all = n * capacity
    sds = jax.ShapeDtypeStruct

    active_gate, slope_gate = silu_parts(output_gate.astype(F32))
    saved = mixer_saved.astype(F32)
    gated = (saved * active_gate).astype(BF16)

    flat = routes.reshape(-1)
    count = flat.shape[0]
    onehot = (flat[:, None] == jnp.arange(n, dtype=jnp.int32)[None, :]).astype(BF16)
    lower = (
        jnp.arange(count, dtype=jnp.int32)[:, None] > jnp.arange(count, dtype=jnp.int32)[None, :]
    ).astype(BF16)
    before = jnp.dot(lower, onehot, preferred_element_type=F32)
    ranks = jnp.sum(before * onehot.astype(F32), axis=1).astype(jnp.int32)
    slots = (flat * capacity + ranks).reshape(tokens, top)
    slot_ids = jnp.arange(slots_all, dtype=jnp.int32)
    hits = [(slots[:, k][None, :] == slot_ids[:, None]) for k in range(top)]
    pick = functools.reduce(jnp.logical_or, hits).astype(BF16)
    slot_weight = sum(
        jnp.sum(jnp.where(hits[k], route_weight[:, k][None, :], 0.0), axis=1) for k in range(top)
    )
    send_input = (
        jnp.dot(pick, layer_input, preferred_element_type=F32)
        .astype(BF16)
        .reshape(n, capacity, d)
    )
    send_cotangent = (
        (jnp.dot(pick, cotangent, preferred_element_type=F32) * slot_weight[:, None])
        .astype(BF16)
        .reshape(n, capacity, d)
    )
    decay_sum = jnp.cumsum(decay_rate, axis=0).T
    heads = decay_sum.shape[0]

    expert_input, expert_cotangent, decays = call(
        functools.partial(dispatch_kernel, n, t),
        1,
        3,
        (
            sds((n, capacity, t * d), BF16),
            sds((n, capacity, t * d), BF16),
            sds((n, heads, tokens), F32),
        ),
        [
            DMA((2, n)),
            DMA((2, n)),
            DMA((2, 3, n)),
            DMA((2, 3, n)),
            DMA((n,)),
            DMA((n,)),
            DMA((3,)),
        ],
        (send_input, send_cotangent, decay_sum),
        "dispatch",
    )
    expert_input = expert_input.reshape(slots_all, t * d)
    expert_cotangent = expert_cotangent.reshape(slots_all, t * d)
    gate_local = gate_weight[0]
    up_local = up_weight[0]
    down_local = down_weight[0]
    pre_gate = jnp.dot(expert_input, gate_local, preferred_element_type=F32)
    pre_up = jnp.dot(expert_input, up_local, preferred_element_type=F32)
    active, slope = silu_parts(pre_gate)
    hidden = (active * pre_up).astype(BF16)
    hidden_grad = lax.dot_general(expert_cotangent, down_local, LAST, preferred_element_type=F32)
    gate_delta = (hidden_grad * pre_up * slope).astype(BF16)
    up_delta = (hidden_grad * active).astype(BF16)
    partial_grad = lax.dot_general(gate_delta, gate_local, LAST, preferred_element_type=F32)
    partial_grad = partial_grad + lax.dot_general(
        up_delta, up_local, LAST, preferred_element_type=F32
    )
    partial_grad = partial_grad.astype(BF16).reshape(n, capacity, t * d)
    block = (n, capacity, d)
    arrived = call(
        functools.partial(combine_kernel, n, t),
        2,
        1,
        sds(block, BF16),
        [
            VMEM((2,) + block, BF16),
            VMEM(block, BF16),
            VMEM(block, BF16),
            VMEM(block, BF16),
            DMA((2,)),
            DMA((2,)),
            DMA((n,)),
            DMA((n,)),
            DMA((n,)),
            DMA((n,)),
            DMA((1,)),
        ],
        (partial_grad,),
        "combine",
    ).reshape(slots_all, d)
    moe_grad = lax.dot_general(pick, arrived, FIRST, preferred_element_type=F32)
    layer_grad = (cotangent.astype(F32) + moe_grad).astype(BF16)
    full_grad = call(
        functools.partial(rows_kernel, n, t),
        3,
        1,
        sds((tokens, t * d), BF16),
        [DMA((3,)), DMA((3,)), DMA((1,))],
        (layer_grad,),
        "rows",
    )
    out_delta = jnp.dot(full_grad, proj_weight, preferred_element_type=F32).astype(BF16)
    outgate_grad = (out_delta.astype(F32) * saved * slope_gate).astype(BF16)
    mixer_delta = (out_delta.astype(F32) * active_gate).astype(BF16)
    width = t * d // n
    by_owner = full_grad.reshape(tokens, n, width).transpose(1, 0, 2)
    length = max(1, n // 2)
    gathered = (mixer_delta, heads_value, gated, state_write, state_read)
    *gathered_all, all_grad = call(
        functools.partial(late_kernel, n, t),
        4,
        6,
        tuple(sds((n,) + x.shape, BF16) for x in gathered) + (sds((n, tokens, width), BF16),),
        [
            DMA((n,)),
            DMA((n,)),
            DMA((3, n)),
            DMA((3, n)),
            DMA((5,)),
            DMA((5,)),
            DMA((5, 2, 2, length)),
            DMA((5, 2, 2, length)),
            DMA((5, 2, length)),
            DMA((5, 2, length)),
            DMA((6,)),
        ],
        gathered + (by_owner,),
        "late",
    )
    all_delta, all_value, all_gated, all_write, all_read = (
        x.reshape(n * tokens, -1) for x in gathered_all
    )

    down_grad = lax.dot_general(hidden, expert_cotangent, FIRST, preferred_element_type=F32)
    gate_grad = lax.dot_general(expert_input, gate_delta, FIRST, preferred_element_type=F32)
    up_grad = lax.dot_general(expert_input, up_delta, FIRST, preferred_element_type=F32)

    state_w = state_write.shape[1]
    proj_grad = lax.dot_general(
        all_grad.reshape(n * tokens, width), all_gated, FIRST, preferred_element_type=F32
    )
    totals = decays[:, :, -1]
    start = jnp.cumsum(totals, axis=0) - totals
    decay_row = (decays + start[:, :, None]).transpose(1, 0, 2)
    decay_here = lax.dynamic_index_in_dim(decay_row, me, axis=1, keepdims=False).T
    chunk = min(4, n) * tokens
    value_grad, write_gradient, read_gradient = call(
        functools.partial(mixer_kernel, chunk),
        None,
        10,
        (sds((tokens, d), BF16), sds((tokens, state_w), BF16), sds((tokens, state_w), BF16)),
        [],
        (
            all_delta,
            all_value,
            all_read,
            all_write,
            decay_row.reshape(heads, n * tokens),
            decay_here,
            mixer_delta,
            heads_value,
            state_read,
            state_write,
        ),
        "mixer",
    )
    return (
        gate_grad.astype(BF16)[None],
        up_grad.astype(BF16)[None],
        down_grad.astype(BF16)[None],
        proj_grad,
        value_grad,
        write_gradient,
        read_gradient,
        outgate_grad,
    )


def solution(mesh):
    split = P("sp", "tp")
    in_specs = (
        split,
        split,
        P("sp", None),
        P("sp", None),
        P("sp", None, "tp"),
        P("sp", None, "tp"),
        P("sp", "tp", None),
        split,
        split,
        split,
        P(None, "tp"),
        split,
        split,
        split,
    )
    out_specs = (
        P("sp", None, "tp"),
        P("sp", None, "tp"),
        P("sp", "tp", None),
        split,
        split,
        split,
        split,
        split,
    )
    return jax.shard_map(
        on_device, mesh=mesh, in_specs=in_specs, out_specs=out_specs, check_vma=False
    )
```

profile of v0, /device:TPU:0, one launch (start us, length us, event | category | flops | bytes accessed | tf_op | source)
XLA Modules:
  0.0 173.9 jit_solution(18227596006571640895)
XLA Ops:
  0.6 0.0 copy-start
  0.6 0.9 copy.53
  1.6 0.1 eq.45
  1.7 0.2 fusion.6
  1.9 0.1 convert_element_type.73
  2.1 0.1 copy.54
  2.1 0.7 multiply_add_fusion
  2.9 1.9 %convolution_convert_fusion.3 = bf16[384,512]{1,0:T(8,128)(2,1)} fusion(bf16[128,512]{1,0:T(8,128)(2,1)} %param.14, s32[128]{0:T(128)S(1)} %get-tuple-element.40, s32[128]{0:T(128)S(1)} %get-tuple-element.39), kind=kOutput, calls=%fused_computation.9 | convolution fusion | flops 50675712 | bytes 525312 | tf_op jit(solution)/shard_map/dot_general | solution.py:499
  4.8 0.8 slice_bitcast_fusion
  5.5 0.2 select_reduce_fusion
  5.7 1.9 %fusion.3 = bf16[384,512]{1,0:T(8,128)(2,1)} fusion(bf16[128,512]{1,0:T(8,128)(2,1)} %param.15, f32[384]{0:T(512)S(1)} %add.44, s32[128]{0:T(128)S(1)} %get-tuple-element.40, s32[128]{0:T(128)S(1)} %get-tuple-element.39), kind=kOutput, calls=%fused_computation.8 | convolution fusion | flops 50872320 | bytes 526848 | tf_op jit(solution)/shard_map/dot_general | solution.py:504
  7.6 0.8 copy.55
  8.4 0.2 reduce_window_sum.22
  8.6 0.7 copy.56
  9.3 0.0 copy-start.2
  9.3 41.0 %dispatch.1 = (bf16[8,48,2048]{2,1,0:T(8,128)(2,1)}, bf16[8,48,2048]{2,1,0:T(8,128)(2,1)}, f32[8,8,128]{2,1,0:T(8,128)}) custom-call(bf16[8,48,512]{2,1,0:T(8,128)(2,1)} %bitcast.74, bf16[8,48,512]{2,1,0:T(8,128)(2,1)} %bitcast.75, f32[8,128]{1,0:T(8,128)} %bitcast.77), custom_call_target="tpu_custom_call" | custom-call | flops 4000000000 | bytes 8000000 | tf_op jit(solution)/shard_map/dispatch/pallas_call | solution.py:436
  50.2 0.0 copy-done.2
  50.2 0.0 copy-start.3
  50.3 0.0 copy-start.10
  50.3 2.1 %fusion.9 = f32[384,256]{1,0:T(8,128)S(1)} fusion(bf16[384,2048]{1,0:T(8,128)(2,1)} %bitcast.78, bf16[1,2048,256]{2,1,0:T(8,128)(2,1)S(1)} %copy-done.2), kind=kOutput, calls=%fused_computation.20 | convolution fusion | flops 402653184 | bytes 3014656 | tf_op jit(solution)/shard_map/dot_general | solution.py:537
  52.4 0.0 copy-done.3
  52.4 0.0 copy-done.10
  52.5 0.0 copy-start.1
  52.5 0.0 copy-start.7
  52.5 0.6 fusion.12
  53.0 0.8 copy-done.1
  53.9 0.3 copy-done.7
  54.2 0.6 multiply_convert_fusion.1
  54.8 1.7 fusion
  56.5 1.7 fusion.1
  58.2 1.7 fusion.2
  60.0 0.6 fusion.7
  60.6 1.8 %add_convert_fusion = bf16[384,2048]{1,0:T(8,128)(2,1)} fusion(f32[384,2048]{1,0:T(8,128)S(1)} %fusion.7, bf16[384,256]{1,0:T(8,128)(2,1)S(1)} %get-tuple-element.32, bf16[1,2048,256]{2,1,0:T(8,128)(2,1)S(1)} %copy-done.3), kind=kOutput, calls=%fused_computation | convolution fusion | flops 404226048 | bytes 5963776 | tf_op jit(solution)/shard_map/dot_general | solution.py:545
  62.4 0.0 copy-start.5
  62.4 25.3 %combine.1 = bf16[8,48,512]{2,1,0:T(8,128)(2,1)} custom-call(bf16[8,48,2048]{2,1,0:T(8,128)(2,1)} %bitcast.71), custom_call_target="tpu_custom_call" | custom-call | flops 4000000000 | bytes 8000000 | tf_op jit(solution)/shard_map/combine/pallas_call | solution.py:436
  87.6 0.0 copy-done.5
  87.6 1.9 %fusion.4.g_ref = bf16[128,512]{1,0:T(8,128)(2,1)} fusion(bf16[384,512]{1,0:T(8,128)(2,1)} %bitcast.73, bf16[128,512]{1,0:T(8,128)(2,1)S(1)} %copy-done.5, s32[128]{0:T(128)S(1)} %get-tuple-element.40, s32[128]{0:T(128)S(1)} %get-tuple-element.39), kind=kOutput, calls=%fused_computation.12 | convolution fusion | flops 50675712 | bytes 656384 | tf_op jit(solution)/shard_map/dot_general | solution.py:571
  89.6 0.0 copy-start.8
  89.6 0.0 copy-start.9
  89.6 8.1 %rows.1 = bf16[128,2048]{1,0:T(8,128)(2,1)} custom-call(bf16[128,512]{1,0:T(8,128)(2,1)} %fusion.4.g_ref), custom_call_target="tpu_custom_call" | custom-call | flops 4000000000 | bytes 8000000 | tf_op jit(solution)/shard_map/rows/pallas_call | solution.py:436
  97.7 0.0 copy-done
  97.7 0.0 copy-done.8
  97.8 0.0 copy-done.9
  97.8 0.0 copy-start.4
  97.8 2.3 %fusion.19 = (bf16[128,512]{1,0:T(8,128)(2,1)}, bf16[128,512]{1,0:T(8,128)(2,1)}, bf16[128,512]{1,0:T(8,128)(2,1)}) fusion(bf16[128,512]{1,0:T(8,128)(2,1)S(1)} %copy-done.8, bf16[128,512]{1,0:T(8,128)(2,1)S(1)} %copy-done.9, bf16[128,2048]{1,0:T(8,128)(2,1)} %rows.1, bf16[2048,512]{1,0:T(8,128)(2,1)S(1)} %copy-done), kind=kOutput, calls=%fused_computation.39 | convolution fusion | flops 269680640 | bytes 3276800 | tf_op jit(solution)/shard_map/dot_general | solution.py:582
  100.1 0.0 copy-done.4
  100.1 0.3 copy.57
  100.4 1.0 copy.58
  101.4 62.0 %late.1 = (bf16[8,128,512]{2,1,0:T(8,128)(2,1)}, bf16[8,128,512]{2,1,0:T(8,128)(2,1)}, bf16[8,128,512]{2,1,0:T(8,128)(2,1)}, bf16[8,128,128]{2,1,0:T(8,128)(2,1)...) custom-call(bf16[128,512]{1,0:T(8,128)(2,1)} %get-tuple-element.35.refs_0_.dl, bf16[128,512]{1,0:T(8,128)(2,1)} %vl.1, ...), custom_call_target="tpu_custom_call" | custom-call | flops 4000000000 | bytes 8000000 | tf_op jit(solution)/shard_map/late/pallas_call | solution.py:436
  163.4 0.0 copy-start.6
  163.4 2.6 %convolution_bitcast_fusion = f32[256,512]{1,0:T(8,128)} fusion(bf16[8,128,256]{2,1,0:T(8,128)(2,1)} %get-tuple-element.22, bf16[8,128,512]{2,1,0:T(8,128)(2,1)} %get-tuple-element.23), kind=kOutput, calls=%fused_computation.10 | convolution fusion | flops 268435456 | bytes 2097152 | tf_op jit(solution)/shard_map/dot_general | solution.py:619
  166.1 0.0 copy-done.6
  166.1 0.2 fusion.40
  166.2 0.7 fusion.58.arow
  166.9 0.1 broadcast_add_fusion
  167.0 0.7 copy.60
  167.7 6.1 %mixer.1 = (bf16[128,512]{1,0:T(8,128)(2,1)}, bf16[128,128]{1,0:T(8,128)(2,1)}, bf16[128,128]{1,0:T(8,128)(2,1)}) custom-call(bf16[1024,512]{1,0:T(8,128)(2,1)} %bitcast.82, bf16[1024,512]{1,0:T(8,128)(2,1)} %bitcast.83, bf16[1024,128]{1,0:T(8,128)(2,1)} %bitcast.85, bf16[1024,128]{1,0:T(8,128)(2,1)} %bitcast.84, f32[8,1024]{1,0:T(8,128)} %fusion.58.arow, ...), custom_call_target="tpu_custom_call" | custom-call | flops 4000000000 | bytes 8000000 | tf_op jit(solution)/shard_map/mixer/pallas_call | solution.py:436
  (4 shorter events, 0.0 us)
Async XLA Ops:
  0.6 97.1 %copy-start = (bf16[2048,512]{1,0:T(8,128)(2,1)S(1)}, bf16[2048,512]{1,0:T(8,128)(2,1)}, u32[]{:S(2)}) copy-start(bf16[2048,512]{1,0:T(8,128)(2,1)} %param.24) | copy-start | bytes 6291460
  9.3 41.0 %copy-start.2 = (bf16[1,2048,256]{2,1,0:T(8,128)(2,1)S(1)}, bf16[1,2048,256]{2,1,0:T(8,128)(2,1)}, u32[]{:S(2)}) copy-start(bf16[1,2048,256]{2,1,0:T(8,128)(2,1)} %param.18) | copy-start | bytes 3145732
  50.2 2.2 %copy-start.3 = (bf16[1,2048,256]{2,1,0:T(8,128)(2,1)S(1)}, bf16[1,2048,256]{2,1,0:T(8,128)(2,1)}, u32[]{:S(2)}) copy-start(bf16[1,2048,256]{2,1,0:T(8,128)(2,1)} %param.19) | copy-start | bytes 3145732
  50.3 2.2 %copy-start.10 = (bf16[8,48,2048]{2,1,0:T(8,128)(2,1)S(1)}, bf16[8,48,2048]{2,1,0:T(8,128)(2,1)}, u32[]{:S(2)}) copy-start(bf16[8,48,2048]{2,1,0:T(8,128)(2,1)} %get-tuple-element.20) | copy-start | bytes 4718596
  52.5 1.4 copy-start.1
  52.5 1.7 copy-start.7
  62.4 25.3 %copy-start.5 = (bf16[128,512]{1,0:T(8,128)(2,1)S(1)}, bf16[128,512]{1,0:T(8,128)(2,1)}, u32[]{:S(2)}) copy-start(bf16[128,512]{1,0:T(8,128)(2,1)} %param.15) | copy-start | bytes 393220
  89.6 8.2 %copy-start.8 = (bf16[128,512]{1,0:T(8,128)(2,1)S(1)}, bf16[128,512]{1,0:T(8,128)(2,1)}, u32[]{:S(2)}) copy-start(bf16[128,512]{1,0:T(8,128)(2,1)} %param.23) | copy-start | bytes 393220
  89.6 8.2 %copy-start.9 = (bf16[128,512]{1,0:T(8,128)(2,1)S(1)}, bf16[128,512]{1,0:T(8,128)(2,1)}, u32[]{:S(2)}) copy-start(bf16[128,512]{1,0:T(8,128)(2,1)} %param.22) | copy-start | bytes 393220
  97.8 2.4 %copy-start.4 = (bf16[128,2048]{1,0:T(8,128)(2,1)S(1)}, bf16[128,2048]{1,0:T(8,128)(2,1)}, u32[]{:S(2)}) copy-start(bf16[128,2048]{1,0:T(8,128)(2,1)} %rows.1) | copy-start | bytes 1572868
  163.4 2.7 %copy-start.6 = (f32[8,8,128]{2,1,0:T(8,128)S(1)}, f32[8,8,128]{2,1,0:T(8,128)}, u32[]{:S(2)}) copy-start(f32[8,8,128]{2,1,0:T(8,128)} %get-tuple-element.28) | copy-start | bytes 98308
where the time goes:
time: 174 us
  Pallas kernels  142 us (82%)
  matrix products  21.8 us (13%)
  local copies, waits for them, and re-layouts  6.68 us (4%)
  other arithmetic  1.99 us (1%)
    pallas_call x5, Pallas kernels, call(): pl.pallas_call(kernel, out_shape=outs, in_specs=[vm] * ins, out_specs=jax...  142 us

commit v1 on v0

--- a/solution.py
+++ b/solution.py
@@ -23,6 +23,26 @@
     return (value * sigma, sigma * (1.0 + value * (1.0 - sigma)))
 
 
+def dot_first(a, b):
+    return lax.dot_general(a, b, FIRST, preferred_element_type=F32)
+
+
+def dot_last(a, b):
+    return lax.dot_general(a, b, LAST, preferred_element_type=F32)
+
+
+def dot(a, b):
+    return jnp.dot(a, b, preferred_element_type=F32)
+
+
+def flip(a, b, n):
+    out, bit = 0, 1
+    while bit < n:
+        out = out + lax.rem(lax.div(a, bit) + lax.div(b, bit), 2) * bit
+        bit *= 2
+    return out
+
+
 class Place:
     def __init__(self, n, t):
         self.n, self.t = n, t
@@ -31,6 +51,9 @@
         self.across = lax.rem(self.tp + t // 2, t)
         self.beside = self.tp + 1 - 2 * lax.rem(self.tp, 2)
         self.cross = lax.rem(self.beside + t // 2, t)
+
+    def mate(self, m):
+        return flip(self.sp, jnp.int32(m), self.n)
 
     def to(self, src, dst, send, recv, sp=None, tp=None):
         return pltpu.make_async_remote_copy(
@@ -67,156 +90,268 @@
     lax.fori_loop(lo, hi, step, 0)
 
 
-def dispatch_kernel(
-    n, t, x_ref, c_ref, a_ref, xo, co, ao, s_a2a, r_a2a, s_sh, r_sh, s_d, r_d, own_sem
+def expert_kernel(
+    n, t, cap,
+    routes, rweight, x_ref, c_ref, a_ref, gate_hbm, up_hbm, down_hbm,
+    full, gate_grad, up_grad, down_grad, ao,
+    snd, got, gate, up, down, pg, pu, hidden, gd, ud, part, pair, summed, other, final, arr, pick,
+    w_sem, s_a2a, r_a2a, s_sh, r_sh, s_d, r_d, s_p, r_p, s_y, r_y, s_b, r_b, s_r, r_r,
 ):
     at = Place(n, t)
-    d = x_ref.shape[2]
+    tokens, d = x_ref.shape
+    top = routes.shape[1]
+    slots = n * cap
+    half = n // 2
+    duo = 2 * cap
     col = lambda tp: pl.ds(pl.multiple_of(tp * d, d), d)
-    sides = ((x_ref, xo), (c_ref, co))
-    at.greet()
-
-    def spread(k, o):
-        src, dst = sides[k]
-        peer = lax.rem(at.sp + o, n)
+
+    loads = [
+        pltpu.make_async_copy(src.at[0], dst, w_sem.at[i])
+        for i, (src, dst) in enumerate(((gate_hbm, gate), (up_hbm, up), (down_hbm, down)))
+    ]
+    for load in loads:
+        load.start()
+
+    barrier = pltpu.get_barrier_semaphore()
+    for tp in (at.across, at.beside):
+        pl.semaphore_signal(barrier, inc=1, device_id=(at.sp, tp), device_id_type=MESH)
+
+    def hello(o):
+        pl.semaphore_signal(
+            barrier, inc=1, device_id=(lax.rem(at.sp + o, n), at.tp), device_id_type=MESH
+        )
+
+    loop(1, n, hello)
+
+    named = routes[...]
+    lanes = lax.broadcasted_iota(jnp.int32, (tokens, n), 1)
+    onehot = [(named[:, k : k + 1] == lanes).astype(F32) for k in range(top)]
+    lower = (
+        lax.broadcasted_iota(jnp.int32, (tokens, tokens), 0)
+        > lax.broadcasted_iota(jnp.int32, (tokens, tokens), 1)
+    ).astype(F32)
+    before = dot(lower.astype(BF16), sum(onehot).astype(BF16))
+    slot_lane = lax.broadcasted_iota(jnp.int32, (tokens, slots), 1)
+    picks = []
+    for k in range(top):
+        rank = jnp.sum(before * onehot[k], axis=1, keepdims=True).astype(jnp.int32)
+        picks.append((named[:, k : k + 1] * cap + rank == slot_lane).astype(F32).astype(BF16))
+    pick[...] = sum(picks)
+    snd[0] = dot_first(pick[...], x_ref[...]).astype(BF16).reshape(n, cap, d)
+    cot = c_ref[...].astype(F32)
+    weights = rweight[...]
+    weighted = [(cot * weights[:, k : k + 1]).astype(BF16) for k in range(top)]
+    snd[1] = dot_first(
+        jnp.concatenate(picks, axis=0), jnp.concatenate(weighted, axis=0)
+    ).astype(BF16).reshape(n, cap, d)
+    for k in (0, 1):
+        got[k, 0, :, col(at.tp)] = snd[k, at.sp]
+    ao[at.sp] = a_ref[...]
+    pl.semaphore_wait(barrier, n + 1)
+
+    def place_of(i):
+        return jnp.where(i < 2, i, n + 1 - i)
+
+    def spread(k, m):
+        mate = at.mate(m)
         return at.to(
-            src.at[peer], dst.at[at.sp, :, col(at.tp)], s_a2a.at[k, o], r_a2a.at[k, o], sp=peer
+            snd.at[k, mate], got.at[k, m, :, col(at.tp)], s_a2a.at[k, m], r_a2a.at[k, m], sp=mate
         )
 
-    def decay(o):
-        peer = lax.rem(at.sp + o, n)
-        return at.to(a_ref, ao.at[at.sp], s_d.at[o], r_d.at[o], sp=peer)
-
-    def share(k, o, j):
-        here = sides[k][1].at[lax.rem(at.sp + n - o, n), :, col(at.across if j == 2 else at.tp)]
+    def decay(m):
+        mate = at.mate(m)
+        return at.to(a_ref, ao.at[at.sp], s_d.at[m], r_d.at[m], sp=mate)
+
+    def share(k, m, j):
+        here = got.at[k, m, :, col(at.across if j == 2 else at.tp)]
         return at.to(
-            here, here, s_sh.at[k, j, o], r_sh.at[k, j, o], tp=at.across if j == 0 else at.beside
+            here, here, s_sh.at[k, j, m], r_sh.at[k, j, m], tp=at.across if j == 0 else at.beside
         )
 
-    owns = [
-        pltpu.make_async_copy(
-            src.at[at.sp], dst.at[at.sp, :, col(at.tp)], own_sem.at[k]
-        )
-        for k, (src, dst) in enumerate(sides)
-    ]
-    owns.append(pltpu.make_async_copy(a_ref, ao.at[at.sp], own_sem.at[2]))
-    for own in owns:
-        own.start()
     for k in (0, 1):
-        loop(1, n, lambda o: spread(k, o).start())
-    loop(1, n, lambda o: decay(o).start())
+        loop(1, n, lambda i: spread(k, place_of(i)).start())
     for k in (0, 1):
-        owns[k].wait()
         share(k, 0, 0).start()
         share(k, 0, 1).start()
-    owns[2].wait()
-    for k in (0, 1):
-
-        def arrive(o):
-            spread(k, o).wait_recv()
-            share(k, o, 0).start()
-            share(k, o, 1).start()
-            share(k, o - 1, 0).wait_recv()
-            share(k, o - 1, 2).start()
-
-        loop(1, n, arrive)
-        share(k, n - 1, 0).wait_recv()
-        share(k, n - 1, 2).start()
-
-    def finish(o):
+    loop(1, n, lambda m: decay(m).start())
+
+    lag = 2
+
+    def forward(q):
+        k, i = lax.div(q, n), lax.rem(q, n)
+        m = place_of(i)
+
+        @pl.when(i > 0)
+        def _():
+            spread(k, m).wait_recv()
+            share(k, m, 0).start()
+            share(k, m, 1).start()
+
+        @pl.when(q >= lag)
+        def _():
+            relay(q - lag)
+
+    def relay(q):
+        k, m = lax.div(q, n), place_of(lax.rem(q, n))
+        share(k, m, 0).wait_recv()
+        share(k, m, 2).start()
+
+    def base_of(j):
+        return jnp.where(j < 1, 0, half - j)
+
+    def settled(k, base):
+        for m in (2 * base, 2 * base + 1):
+            share(k, m, 1).wait_recv()
+            share(k, m, 2).wait_recv()
+
+    def rows_of(base):
+        return pl.ds(pl.multiple_of(base * duo, duo), duo)
+
+    def ahead(j):
+        base = base_of(j)
+        settled(0, base)
+        rows = rows_of(base)
+        inputs = got[0, pl.ds(2 * base, 2)].reshape(duo, t * d)
+        pg[rows, :] = dot(inputs, gate[...])
+        pu[rows, :] = dot(inputs, up[...])
+
+    def behind(j):
+        base = base_of(j)
+        settled(1, base)
+        rows = rows_of(base)
+        sent = got[1, pl.ds(2 * base, 2)].reshape(duo, t * d)
+        grad = dot_last(sent, down[...])
+        active, slope = silu_parts(pg[rows, :])
+        ups = pu[rows, :]
+        hidden[rows, :] = (active * ups).astype(BF16)
+        gd[rows, :] = (grad * ups * slope).astype(BF16)
+        ud[rows, :] = (grad * active).astype(BF16)
+
+    loop(1, n, forward)
+    for load in loads:
+        load.wait()
+
+    def second(j):
+        forward(n + 2 * j)
+        forward(n + 2 * j + 1)
+        ahead(j)
+
+        @pl.when(j > 0)
+        def _():
+            behind(j - 1)
+
+    loop(0, half, second)
+    loop(2 * n - lag, 2 * n, relay)
+    behind(half - 1)
+
+    def halves(m, k):
+        c = at.cross if k == 0 else at.beside
+        return at.to(
+            part.at[m, :, col(c)], pair.at[k, m], s_p.at[k, m], r_p.at[k, m], tp=at.beside
+        )
+
+    def over(m):
+        return at.to(summed.at[m], other.at[m], s_y.at[m], r_y.at[m], tp=at.across)
+
+    def back(m):
+        return at.to(final.at[m], arr.at[at.sp], s_b.at[m], r_b.at[m], sp=at.mate(m))
+
+    def produce(jj):
+        base = half - 1 - jj
+        rows = rows_of(base)
+        for c in range(t):
+            cols = slice(c * d, (c + 1) * d)
+            value = dot_last(gd[rows, :], gate[cols, :]) + dot_last(ud[rows, :], up[cols, :])
+            part[pl.ds(2 * base, 2), :, cols] = value.astype(BF16).reshape(2, cap, d)
+        for m in (2 * base + 1, 2 * base):
+            for k in (0, 1):
+                halves(m, k).start()
+
+    def pass_over(jj):
+        base = half - 1 - jj
+        for m in (2 * base + 1, 2 * base):
+            halves(m, 0).wait_recv()
+            summed[m] = (
+                part[m, :, col(at.across)].astype(F32) + pair[0, m].astype(F32)
+            ).astype(BF16)
+            over(m).start()
+
+    def total(jj):
+        base = half - 1 - jj
+        for m in (2 * base + 1, 2 * base):
+            halves(m, 1).wait_recv()
+            over(m).wait_recv()
+            final[m] = (
+                part[m, :, col(at.tp)].astype(F32) + pair[1, m].astype(F32) + other[m].astype(F32)
+            ).astype(BF16)
+
+            @pl.when(m > 0)
+            def _():
+                back(m).start()
+
+    def first_turn(jj):
+        produce(jj)
+
+        @pl.when(jj > 0)
+        def _():
+            pass_over(jj - 1)
+
+    def weight_grads(c):
+        cols = pl.ds(pl.multiple_of(c * d, d), d)
+        inputs = got[0, :, :, cols].reshape(slots, d)
+        gate_grad[cols, :] = dot_first(inputs, gd[...]).astype(BF16)
+        up_grad[cols, :] = dot_first(inputs, ud[...]).astype(BF16)
+        sent = got[1, :, :, cols].reshape(slots, d)
+        down_grad[:, cols] = dot_first(hidden[...], sent).astype(BF16)
+
+    loop(0, half, first_turn)
+    pass_over(half - 1)
+
+    def last_turn(jj):
+        total(jj)
+
+        @pl.when(jj < t)
+        def _():
+            weight_grads(jj)
+
+    loop(0, half, last_turn)
+    for c in range(half, t):
+        weight_grads(c)
+    arr[at.sp] = final[0]
+    loop(1, n, lambda i: back(n - i).wait_recv())
+
+    moe_grad = dot(pick[...], arr[...].reshape(slots, d))
+    full[:, col(at.tp)] = (c_ref[...].astype(F32) + moe_grad).astype(BF16)
+
+    def rows_to(j):
+        here = full.at[:, col(at.across if j == 2 else at.tp)]
+        return at.to(here, here, s_r.at[j], r_r.at[j], tp=at.across if j == 0 else at.beside)
+
+    rows_to(0).start()
+    rows_to(1).start()
+    rows_to(0).wait_recv()
+    rows_to(2).start()
+
+    def finish(m):
         for k in (0, 1):
-            share(k, o, 1).wait_recv()
-            share(k, o, 2).wait_recv()
             for j in (0, 1, 2):
-                share(k, o, j).wait_send()
+                share(k, m, j).wait_send()
+            halves(m, k).wait_send()
+        over(m).wait_send()
 
     loop(0, n, finish)
 
-    def finish_spread(o):
+    def finish_sp(m):
         for k in (0, 1):
-            spread(k, o).wait_send()
-        decay(o).wait()
-
-    loop(1, n, finish_spread)
-
-
-def combine_kernel(n, t, p_ref, out, pair, summed, other, final, s_p, r_p, s_y, r_y, s_a, r_a, own):
-    at = Place(n, t)
-    d = out.shape[2]
-    col = lambda tp: pl.ds(pl.multiple_of(tp * d, d), d)
-    at.greet()
-    halves = [
-        at.to(p_ref.at[:, :, col(c)], pair.at[k], s_p.at[k], r_p.at[k], tp=at.beside)
-        for k, c in enumerate((at.cross, at.beside))
-    ]
-    for half in halves:
-        half.start()
-
-    def over(o):
-        b = lax.rem(at.sp + o, n)
-        return at.to(summed.at[b], other.at[b], s_y.at[o], r_y.at[o], tp=at.across)
-
-    def back(o):
-        b = lax.rem(at.sp + o, n)
-        return at.to(final.at[b], out.at[at.sp], s_a.at[o], r_a.at[o], sp=b)
-
-    halves[0].wait_recv()
-
-    def add_pair(o):
-        b = lax.rem(at.sp + o, n)
-        summed[b] = (
-            p_ref[b, :, col(at.across)].astype(F32) + pair[0, b].astype(F32)
-        ).astype(BF16)
-        over(o).start()
-
-    def turn(i):
-        o = i + 1
-        add_pair(lax.rem(o, n))
-
-    loop(0, n, turn)
-    halves[1].wait_recv()
-
-    def total(o):
-        b = lax.rem(at.sp + o, n)
-        over(o).wait_recv()
-        final[b] = (
-            p_ref[b, :, col(at.tp)].astype(F32) + pair[1, b].astype(F32) + other[b].astype(F32)
-        ).astype(BF16)
-
-    def total_and_send(o):
-        total(o)
-        back(o).start()
-
-    loop(1, n, total_and_send)
-    total(0)
-    mine = pltpu.make_async_copy(final.at[at.sp], out.at[at.sp], own.at[0])
-    mine.start()
-    mine.wait()
-    for half in halves:
-        half.wait_send()
-    loop(0, n, lambda o: over(o).wait_send())
-    loop(1, n, lambda o: back(o).wait())
-
-
-def rows_kernel(n, t, g_ref, out, s_sh, r_sh, own):
-    at = Place(n, t)
-    d = g_ref.shape[1]
-    col = lambda tp: pl.ds(pl.multiple_of(tp * d, d), d)
-    at.greet(sp_too=False)
-    mine = pltpu.make_async_copy(g_ref, out.at[:, col(at.tp)], own.at[0])
-    mine.start()
-    first = at.to(g_ref, out.at[:, col(at.tp)], s_sh.at[0], r_sh.at[0], tp=at.across)
-    side = at.to(g_ref, out.at[:, col(at.tp)], s_sh.at[1], r_sh.at[1], tp=at.beside)
-    first.start()
-    side.start()
-    here = out.at[:, col(at.across)]
-    onward = at.to(here, here, s_sh.at[2], r_sh.at[2], tp=at.beside)
-    first.wait_recv()
-    onward.start()
-    mine.wait()
-    side.wait()
-    first.wait_send()
-    onward.wait()
+            spread(k, m).wait_send()
+        back(m).wait_send()
+        decay(m).wait()
+
+    loop(1, n, finish_sp)
+    rows_to(1).wait_recv()
+    rows_to(2).wait_recv()
+    for j in (0, 1, 2):
+        rows_to(j).wait_send()
 
 
 def late_kernel(n, t, *refs):
@@ -431,12 +566,15 @@
         rg[:, g * STATE : (g + 1) * STATE] = rg_sum[g].astype(BF16)
 
 
-def call(kernel, ident, ins, outs, scratch, operands, name):
+def call(kernel, ident, ins, outs, scratch, operands, name, any_from=None):
     vm = pl.BlockSpec(memory_space=pltpu.VMEM)
     return pl.pallas_call(
         kernel,
         out_shape=outs,
-        in_specs=[vm] * ins,
+        in_specs=[
+            vm if any_from is None or i < any_from else pl.BlockSpec(memory_space=pl.ANY)
+            for i in range(len(operands))
+        ],
         out_specs=jax.tree.map(lambda _: vm, outs),
         scratch_shapes=scratch,
         compiler_params=pltpu.CompilerParams(
@@ -472,112 +610,65 @@
     me = lax.axis_index("sp")
     tokens, d = layer_input.shape
     top = routes.shape[1]
-    capacity = max(2, 3 * tokens * top // (2 * n))
+    capacity = -(-max(2, 3 * tokens * top // (2 * n)) // 16) * 16
     slots_all = n * capacity
     sds = jax.ShapeDtypeStruct
 
     active_gate, slope_gate = silu_parts(output_gate.astype(F32))
     saved = mixer_saved.astype(F32)
     gated = (saved * active_gate).astype(BF16)
-
-    flat = routes.reshape(-1)
-    count = flat.shape[0]
-    onehot = (flat[:, None] == jnp.arange(n, dtype=jnp.int32)[None, :]).astype(BF16)
-    lower = (
-        jnp.arange(count, dtype=jnp.int32)[:, None] > jnp.arange(count, dtype=jnp.int32)[None, :]
-    ).astype(BF16)
-    before = jnp.dot(lower, onehot, preferred_element_type=F32)
-    ranks = jnp.sum(before * onehot.astype(F32), axis=1).astype(jnp.int32)
-    slots = (flat * capacity + ranks).reshape(tokens, top)
-    slot_ids = jnp.arange(slots_all, dtype=jnp.int32)
-    hits = [(slots[:, k][None, :] == slot_ids[:, None]) for k in range(top)]
-    pick = functools.reduce(jnp.logical_or, hits).astype(BF16)
-    slot_weight = sum(
-        jnp.sum(jnp.where(hits[k], route_weight[:, k][None, :], 0.0), axis=1) for k in range(top)
-    )
-    send_input = (
-        jnp.dot(pick, layer_input, preferred_element_type=F32)
-        .astype(BF16)
-        .reshape(n, capacity, d)
-    )
-    send_cotangent = (
-        (jnp.dot(pick, cotangent, preferred_element_type=F32) * slot_weight[:, None])
-        .astype(BF16)
-        .reshape(n, capacity, d)
-    )
     decay_sum = jnp.cumsum(decay_rate, axis=0).T
     heads = decay_sum.shape[0]
-
-    expert_input, expert_cotangent, decays = call(
-        functools.partial(dispatch_kernel, n, t),
+    hid = gate_weight.shape[2]
+    block = (n, capacity, d)
+    full_grad, gate_grad, up_grad, down_grad, decays = call(
+        functools.partial(expert_kernel, n, t, capacity),
         1,
-        3,
+        5,
         (
-            sds((n, capacity, t * d), BF16),
-            sds((n, capacity, t * d), BF16),
+            sds((tokens, t * d), BF16),
+            sds((t * d, hid), BF16),
+            sds((t * d, hid), BF16),
+            sds((hid, t * d), BF16),
             sds((n, heads, tokens), F32),
         ),
         [
+            VMEM((2,) + block, BF16),
+            VMEM((2, n, capacity, t * d), BF16),
+            VMEM((t * d, hid), BF16),
+            VMEM((t * d, hid), BF16),
+            VMEM((hid, t * d), BF16),
+            VMEM((slots_all, hid), F32),
+            VMEM((slots_all, hid), F32),
+            VMEM((slots_all, hid), BF16),
+            VMEM((slots_all, hid), BF16),
+            VMEM((slots_all, hid), BF16),
+            VMEM((n, capacity, t * d), BF16),
+            VMEM((2,) + block, BF16),
+            VMEM(block, BF16),
+            VMEM(block, BF16),
+            VMEM(block, BF16),
+            VMEM(block, BF16),
+            VMEM((tokens, slots_all), BF16),
+            DMA((3,)),
             DMA((2, n)),
             DMA((2, n)),
             DMA((2, 3, n)),
             DMA((2, 3, n)),
             DMA((n,)),
             DMA((n,)),
-            DMA((3,)),
-        ],
-        (send_input, send_cotangent, decay_sum),
-        "dispatch",
-    )
-    expert_input = expert_input.reshape(slots_all, t * d)
-    expert_cotangent = expert_cotangent.reshape(slots_all, t * d)
-    gate_local = gate_weight[0]
-    up_local = up_weight[0]
-    down_local = down_weight[0]
-    pre_gate = jnp.dot(expert_input, gate_local, preferred_element_type=F32)
-    pre_up = jnp.dot(expert_input, up_local, preferred_element_type=F32)
-    active, slope = silu_parts(pre_gate)
-    hidden = (active * pre_up).astype(BF16)
-    hidden_grad = lax.dot_general(expert_cotangent, down_local, LAST, preferred_element_type=F32)
-    gate_delta = (hidden_grad * pre_up * slope).astype(BF16)
-    up_delta = (hidden_grad * active).astype(BF16)
-    partial_grad = lax.dot_general(gate_delta, gate_local, LAST, preferred_element_type=F32)
-    partial_grad = partial_grad + lax.dot_general(
-        up_delta, up_local, LAST, preferred_element_type=F32
-    )
-    partial_grad = partial_grad.astype(BF16).reshape(n, capacity, t * d)
-    block = (n, capacity, d)
-    arrived = call(
-        functools.partial(combine_kernel, n, t),
-        2,
-        1,
-        sds(block, BF16),
-        [
-            VMEM((2,) + block, BF16),
-            VMEM(block, BF16),
-            VMEM(block, BF16),
-            VMEM(block, BF16),
-            DMA((2,)),
-            DMA((2,)),
+            DMA((2, n)),
+            DMA((2, n)),
             DMA((n,)),
             DMA((n,)),
             DMA((n,)),
             DMA((n,)),
-            DMA((1,)),
+            DMA((3,)),
+            DMA((3,)),
         ],
-        (partial_grad,),
-        "combine",
-    ).reshape(slots_all, d)
-    moe_grad = lax.dot_general(pick, arrived, FIRST, preferred_element_type=F32)
-    layer_grad = (cotangent.astype(F32) + moe_grad).astype(BF16)
-    full_grad = call(
-        functools.partial(rows_kernel, n, t),
-        3,
-        1,
-        sds((tokens, t * d), BF16),
-        [DMA((3,)), DMA((3,)), DMA((1,))],
-        (layer_grad,),
-        "rows",
+        (routes, route_weight, layer_input, cotangent, decay_sum, gate_weight, up_weight, down_weight),
+        "experts",
+        any_from=5,
     )
     out_delta = jnp.dot(full_grad, proj_weight, preferred_element_type=F32).astype(BF16)
     outgate_grad = (out_delta.astype(F32) * saved * slope_gate).astype(BF16)
@@ -611,10 +702,6 @@
         x.reshape(n * tokens, -1) for x in gathered_all
     )
 
-    down_grad = lax.dot_general(hidden, expert_cotangent, FIRST, preferred_element_type=F32)
-    gate_grad = lax.dot_general(expert_input, gate_delta, FIRST, preferred_element_type=F32)
-    up_grad = lax.dot_general(expert_input, up_delta, FIRST, preferred_element_type=F32)
-
     state_w = state_write.shape[1]
     proj_grad = lax.dot_general(
         all_grad.reshape(n * tokens, width), all_gated, FIRST, preferred_element_type=F32
@@ -645,9 +732,9 @@
         "mixer",
     )
     return (
-        gate_grad.astype(BF16)[None],
-        up_grad.astype(BF16)[None],
-        down_grad.astype(BF16)[None],
+        gate_grad[None],
+        up_grad[None],
+        down_grad[None],
         proj_grad,
         value_grad,
         write_gradient,

time: 174 us -> 145 us (0.83)
  matrix products: 21.8 us -> 3.59 us
  Pallas kernels: 142 us -> 130 us
  local copies, waits for them, and re-layouts: 6.68 us -> 9.4 us
    dot_general x12 -> x0, matrix products: 16.9 us -> none  [the longest x1 2.13 us: on_device(): pre_gate = jnp.dot(expert_input, gate_local, preferred_element_type=F32)]
    pallas_call x5 -> x3, Pallas kernels: 142 us -> 130 us  [call(): pl.pallas_call(kernel, out_shape=outs, in_specs=[vm if any_from is None o...]
    unnamed x24 -> x26, local copies, waits for them, and re-layouts: 2.91 us -> 6.71 us
where the time goes in v1:
time: 145 us; the launch traced here: 144 us
  Pallas kernels  130 us (90%)
  local copies, waits for them, and re-layouts  9.4 us (6%)
  matrix products  3.59 us (2%)
    pallas_call x3, Pallas kernels, call(): pl.pallas_call(kernel, out_shape=outs, in_specs=[vm if any_from is None o...  130 us
    unnamed x26, local copies, waits for them, and re-layouts  6.71 us

profile of v1, /device:TPU:0, one launch (start us, length us, event | category | flops | bytes accessed | tf_op | source)
XLA Modules:
  0.0 144.4 jit_solution(16098631128911754845)
XLA Ops:
  0.6 0.0 copy-start
  0.6 0.9 copy.28
  1.6 0.2 reduce_window_sum.22
  1.8 0.7 copy.29
  2.4 1.4 copy.30.routes
  3.8 1.4 copy.31.rweight
  5.2 0.0 copy-start.8
  5.2 0.0 copy-start.9
  5.2 62.4 %experts.1 = (bf16[128,2048]{1,0:T(8,128)(2,1)}, bf16[2048,256]{1,0:T(8,128)(2,1)}, bf16[2048,256]{1,0:T(8,128)(2,1)}, bf16[256,2048]{1,0:T(8,128)(2,1)}, f32[8,8,128]{2,1,0:T(8,128)}) custom-call(s32[128,2]{1,0:T(8,128)} %copy.30.routes, f32[128,2]{1,0:T(8,128)} %copy.31.rweight, bf16[128,512]{1,0:T(8,128)(2,1)} %x_ref.1, bf16[128,512]{1,0:T(8,128)(2,1)} %c_ref.1, ...), custom_call_target="tpu_custom_call" | custom-call | flops 4000000000 | bytes 8000000 | tf_op jit(solution)/shard_map/experts/pallas_call | solution.py:571
  67.6 0.0 copy-start.5
  67.6 0.0 copy-done
  67.6 0.0 copy-done.8
  67.6 0.0 copy-done.9
  67.7 2.3 %fusion.3 = (bf16[128,512]{1,0:T(8,128)(2,1)}, bf16[128,512]{1,0:T(8,128)(2,1)}, bf16[128,512]{1,0:T(8,128)(2,1)}) fusion(bf16[128,512]{1,0:T(8,128)(2,1)S(1)} %copy-done.8, bf16[128,512]{1,0:T(8,128)(2,1)S(1)} %copy-done.9, bf16[128,2048]{1,0:T(8,128)(2,1)} %get-tuple-element.25, bf16[2048,512]{1,0:T(8,128)(2,1)S(1)} %copy-done), kind=kOutput, calls=%fused_computation.11 | convolution fusion | flops 269680640 | bytes 3276800 | tf_op jit(solution)/shard_map/dot_general | solution.py:673
  70.0 0.0 copy-done.5
  70.0 0.3 copy.32
  70.3 1.0 copy.33
  71.3 0.0 copy-start.7
  71.3 61.0 %late.1 = (bf16[8,128,512]{2,1,0:T(8,128)(2,1)}, bf16[8,128,512]{2,1,0:T(8,128)(2,1)}, bf16[8,128,512]{2,1,0:T(8,128)(2,1)}, bf16[8,128,128]{2,1,0:T(8,128)(2,1)...) custom-call(bf16[128,512]{1,0:T(8,128)(2,1)} %get-tuple-element.37.refs_0_.dl, bf16[128,512]{1,0:T(8,128)(2,1)} %vl.1, ...), custom_call_target="tpu_custom_call" | custom-call | flops 4000000000 | bytes 8000000 | tf_op jit(solution)/shard_map/late/pallas_call | solution.py:571
  132.3 0.0 copy-done.7
  132.3 0.2 fusion.10
  132.4 0.1 broadcast_add_fusion
  132.5 0.7 copy.35
  133.2 0.7 fusion.15.arow
  133.9 0.0 copy-start.4
  133.9 0.0 copy-start.6
  133.9 6.2 %mixer.1 = (bf16[128,512]{1,0:T(8,128)(2,1)}, bf16[128,128]{1,0:T(8,128)(2,1)}, bf16[128,128]{1,0:T(8,128)(2,1)}) custom-call(bf16[1024,512]{1,0:T(8,128)(2,1)} %bitcast.30, bf16[1024,512]{1,0:T(8,128)(2,1)} %bitcast.31, bf16[1024,128]{1,0:T(8,128)(2,1)} %bitcast.33, bf16[1024,128]{1,0:T(8,128)(2,1)} %bitcast.32, f32[8,1024]{1,0:T(8,128)} %fusion.15.arow, ...), custom_call_target="tpu_custom_call" | custom-call | flops 4000000000 | bytes 8000000 | tf_op jit(solution)/shard_map/mixer/pallas_call | solution.py:571
  140.2 0.0 copy-start.3
  140.2 0.0 copy-done.4
  140.2 0.0 copy-done.6
  140.2 0.0 copy-start.2
  140.2 1.3 convolution_bitcast_fusion
  141.4 0.0 copy-done.3
  141.4 0.0 copy-start.1
  141.4 1.0 copy.40
  142.4 0.0 copy-done.2
  142.4 1.0 copy.41
  143.4 0.0 copy-done.1
  143.4 1.0 copy.42
  (1 shorter events, 0.0 us)
Async XLA Ops:
  0.6 67.0 %copy-start = (bf16[2048,512]{1,0:T(8,128)(2,1)S(1)}, bf16[2048,512]{1,0:T(8,128)(2,1)}, u32[]{:S(2)}) copy-start(bf16[2048,512]{1,0:T(8,128)(2,1)} %param.24) | copy-start | bytes 6291460
  5.2 62.4 %copy-start.8 = (bf16[128,512]{1,0:T(8,128)(2,1)S(1)}, bf16[128,512]{1,0:T(8,128)(2,1)}, u32[]{:S(2)}) copy-start(bf16[128,512]{1,0:T(8,128)(2,1)} %param.23) | copy-start | bytes 393220
  5.2 62.4 %copy-start.9 = (bf16[128,512]{1,0:T(8,128)(2,1)S(1)}, bf16[128,512]{1,0:T(8,128)(2,1)}, u32[]{:S(2)}) copy-start(bf16[128,512]{1,0:T(8,128)(2,1)} %param.22) | copy-start | bytes 393220
  67.6 2.4 %copy-start.5 = (bf16[128,2048]{1,0:T(8,128)(2,1)S(1)}, bf16[128,2048]{1,0:T(8,128)(2,1)}, u32[]{:S(2)}) copy-start(bf16[128,2048]{1,0:T(8,128)(2,1)} %get-tuple-element.25) | copy-start | bytes 1572868
  71.3 61.0 %copy-start.7 = (f32[8,8,128]{2,1,0:T(8,128)S(1)}, f32[8,8,128]{2,1,0:T(8,128)}, u32[]{:S(2)}) copy-start(f32[8,8,128]{2,1,0:T(8,128)} %get-tuple-element.32) | copy-start | bytes 98308
  133.9 6.2 %copy-start.4 = (bf16[8,128,512]{2,1,0:T(8,128)(2,1)S(1)}, bf16[8,128,512]{2,1,0:T(8,128)(2,1)}, u32[]{:S(2)}) copy-start(bf16[8,128,512]{2,1,0:T(8,128)(2,1)} %get-tuple-element.27) | copy-start | bytes 3145732
  133.9 6.2 %copy-start.6 = (bf16[8,128,256]{2,1,0:T(8,128)(2,1)S(1)}, bf16[8,128,256]{2,1,0:T(8,128)(2,1)}, u32[]{:S(2)}) copy-start(bf16[8,128,256]{2,1,0:T(8,128)(2,1)} %get-tuple-element.26) | copy-start | bytes 1572868
  140.2 1.3 copy-start.3
  140.2 2.2 %copy-start.2 = (bf16[2048,256]{1,0:T(8,128)(2,1)S(1)}, bf16[2048,256]{1,0:T(8,128)(2,1)}, u32[]{:S(2)}) copy-start(bf16[2048,256]{1,0:T(8,128)(2,1)} %get-tuple-element.23) | copy-start | bytes 3145732
  141.4 1.9 %copy-start.1 = (bf16[256,2048]{1,0:T(8,128)(2,1)S(1)}, bf16[256,2048]{1,0:T(8,128)(2,1)}, u32[]{:S(2)}) copy-start(bf16[256,2048]{1,0:T(8,128)(2,1)} %get-tuple-element.24) | copy-start | bytes 3145732

commit v2 on v1

v2 whole, which is shorter than its diff:
```python
import functools

import jax
import jax.numpy as jnp
from jax import lax
from jax.experimental import pallas as pl
from jax.experimental.pallas import tpu as pltpu
from jax.sharding import PartitionSpec as P

HEAD_DIM = 64
STATE = 128
MESH = pl.DeviceIdType.MESH
LAST = (((1,), (1,)), ((), ()))
FIRST = (((0,), (0,)), ((), ()))
F32 = jnp.float32
BF16 = jnp.bfloat16
VMEM = pltpu.VMEM
DMA = pltpu.SemaphoreType.DMA


def silu_parts(value):
    sigma = jax.nn.sigmoid(value)
    return (value * sigma, sigma * (1.0 + value * (1.0 - sigma)))


def dot_first(a, b):
    return lax.dot_general(a, b, FIRST, preferred_element_type=F32)


def dot_last(a, b):
    return lax.dot_general(a, b, LAST, preferred_element_type=F32)


def dot(a, b):
    return jnp.dot(a, b, preferred_element_type=F32)


def exact(a, b, dims=(((1,), (0,)), ((), ()))):
    return lax.dot_general(
        a, b, dims, precision=lax.Precision.HIGHEST, preferred_element_type=F32
    )


def flip(a, b, n):
    out, bit = 0, 1
    while bit < n:
        out = out + lax.rem(lax.div(a, bit) + lax.div(b, bit), 2) * bit
        bit *= 2
    return out


class Place:
    def __init__(self, n, t):
        self.n, self.t = n, t
        self.sp = lax.axis_index("sp")
        self.tp = lax.axis_index("tp")
        self.across = lax.rem(self.tp + t // 2, t)
        self.beside = self.tp + 1 - 2 * lax.rem(self.tp, 2)
        self.cross = lax.rem(self.beside + t // 2, t)

    def mate(self, m):
        return flip(self.sp, jnp.int32(m), self.n)

    def to(self, src, dst, send, recv, sp=None, tp=None):
        return pltpu.make_async_remote_copy(
            src_ref=src,
            dst_ref=dst,
            send_sem=send,
            recv_sem=recv,
            device_id=(self.sp if sp is None else sp, self.tp if tp is None else tp),
            device_id_type=MESH,
        )


def loop(lo, hi, body):
    def step(i, carry):
        body(i)
        return carry

    lax.fori_loop(lo, hi, step, 0)


def layer_kernel(
    n, t, cap,
    routes, rweight, rates, x_ref, c_ref, vl, og, ms, wl, rl, gate_hbm, up_hbm, down_hbm, pw_hbm,
    gate_out, up_out, down_out, proj, vg, wg, rg, outg,
    snd, got, gate, up, down, pw, pg, pu, hidden, gd, ud, part, pair, summed, other, final, arr,
    pick, gate_grad, up_grad, down_grad, trow, acol, ends, twins, joint, lined, lowhigh, delta,
    ga, full, by, gall,
    w_sem, o_sem, s_a2a, r_a2a, s_sh, r_sh, s_d, r_d, s_p, r_p, s_y, r_y, s_b, r_b, s_r, r_r,
    s_t1, r_t1, s_t2, r_t2, s_t3, r_t3, s_z, r_z, s_l, r_l, s_ls, r_ls, s_x, r_x, s_g, r_g,
    s_gs, r_gs,
):
    at = Place(n, t)
    tokens, d = x_ref.shape
    top = routes.shape[0]
    slots = n * cap
    half = n // 2
    duo = 2 * cap
    heads = rates.shape[0]
    per = heads * STATE // wl.shape[1]
    span = per * HEAD_DIM
    groups = heads // per
    z = lax.div(at.sp, 2)
    bit = lax.rem(at.sp, 2)
    twin = at.sp + 1 - 2 * bit
    col = lambda tp: pl.ds(pl.multiple_of(tp * d, d), d)
    hcol = lambda b: pl.ds(pl.multiple_of(b * (d // 2), d // 2), d // 2)

    weights_in = ((gate_hbm.at[0], gate), (up_hbm.at[0], up), (down_hbm.at[0], down), (pw_hbm, pw))
    loads = [
        pltpu.make_async_copy(src, dst, w_sem.at[i]) for i, (src, dst) in enumerate(weights_in)
    ]
    for load in loads:
        load.start()

    barrier = pltpu.get_barrier_semaphore()
    for tp in (at.across, at.beside):
        pl.semaphore_signal(barrier, inc=1, device_id=(at.sp, tp), device_id_type=MESH)

    def hello(o):
        pl.semaphore_signal(
            barrier, inc=1, device_id=(lax.rem(at.sp + o, n), at.tp), device_id_type=MESH
        )

    loop(1, n, hello)

    row_id = lax.broadcasted_iota(jnp.int32, (tokens, tokens), 0)
    col_id = lax.broadcasted_iota(jnp.int32, (tokens, tokens), 1)
    eye = (row_id == col_id).astype(F32)
    named = exact(eye, routes[...].astype(F32), LAST)
    weights = exact(eye, rweight[...], LAST)
    lanes = lax.broadcasted_iota(jnp.int32, (tokens, n), 1).astype(F32)
    onehot = [(named[:, k : k + 1] == lanes).astype(F32) for k in range(top)]
    lower = (row_id > col_id).astype(F32)
    before = dot(lower.astype(BF16), sum(onehot).astype(BF16))
    slot_lane = lax.broadcasted_iota(jnp.int32, (tokens, slots), 1).astype(F32)
    picks = []
    for k in range(top):
        rank = jnp.sum(before * onehot[k], axis=1, keepdims=True)
        picks.append((named[:, k : k + 1] * cap + rank == slot_lane).astype(F32).astype(BF16))
    pick[...] = sum(picks)
    snd[0] = dot_first(pick[...], x_ref[...]).astype(BF16).reshape(n, cap, d)
    cot = c_ref[...].astype(F32)
    weighted = [(cot * weights[:, k : k + 1]).astype(BF16) for k in range(top)]
    snd[1] = dot_first(
        jnp.concatenate(picks, axis=0), jnp.concatenate(weighted, axis=0)
    ).astype(BF16).reshape(n, cap, d)
    for k in (0, 1):
        got[k, 0, :, col(at.tp)] = snd[k, at.sp]
    pl.semaphore_wait(barrier, n + 1)


    def to_columns(value):
        lane = lax.broadcasted_iota(jnp.int32, (heads, d), 1)
        lead = lax.broadcasted_iota(jnp.int32, (heads, d), 0) * HEAD_DIM
        spread_heads = jnp.logical_and(lane >= lead, lane < lead + HEAD_DIM).astype(F32)
        return exact(value, spread_heads, FIRST)

    def prepare():
        upto = (row_id >= col_id).astype(F32)
        acol[...] = exact(upto, to_columns(rates[...]))
        trow[at.sp] = acol[tokens - 1 : tokens, :]
        ga[at.sp] = (
            ms[...].astype(F32) * silu_parts(og[...].astype(F32))[0]
        ).astype(BF16)

    def states(kind, left, right):
        a = acol[...]
        value = right[...].astype(F32)
        for i, fade in enumerate((jnp.exp(a - a[tokens - 1 : tokens, :]), jnp.exp(-a))):
            faded = (value * fade).astype(BF16)
            for g in range(groups):
                ends[kind, i, :, g * span : (g + 1) * span] = dot_first(
                    left[:, g * STATE : (g + 1) * STATE], faded[:, g * span : (g + 1) * span]
                ).astype(BF16)

    def totals(m):
        mate = at.mate(m)
        return at.to(trow.at[at.sp], trow.at[at.sp], s_d.at[m], r_d.at[m], sp=mate)

    def twin_first(kind):
        cols = hcol(1 - bit)
        return at.to(
            ends.at[kind, :, :, cols], twins.at[kind, :, :, cols], s_t1.at[kind], r_t1.at[kind],
            sp=twin,
        )

    def twin_rest(kind):
        cols = hcol(bit)
        return at.to(
            ends.at[kind, bit, :, cols], twins.at[kind, bit, :, cols], s_t2.at[kind],
            r_t2.at[kind], sp=twin,
        )

    def along(kind, o):
        there = lax.rem(z + o, half)
        return at.to(
            joint.at[kind, jnp.where(there > z, 0, 1)], lined.at[kind, z], s_z.at[kind, o],
            r_z.at[kind, o], sp=there * 2 + bit,
        )

    def twin_last(kind):
        here = lowhigh.at[kind, :, :, hcol(bit)]
        return at.to(here, here, s_t3.at[kind], r_t3.at[kind], sp=twin)

    def join(kind):
        cols = hcol(bit)
        mine = jnp.exp(-trow[at.sp, :, cols])
        his = jnp.exp(-trow[twin, :, cols])
        second = (bit == 1).astype(F32)
        keep_end = second + (1.0 - second) * his
        his_end = (1.0 - second) + second * mine
        keep_start = (1.0 - second) + second * his
        his_start = second + (1.0 - second) * mine
        own = ends[kind, :, :, cols].astype(F32)
        got_twin = twins[kind, :, :, cols].astype(F32)
        joint[kind, 0] = (own[0] * keep_end + got_twin[0] * his_end).astype(BF16)
        joint[kind, 1] = (own[1] * keep_start + got_twin[1] * his_start).astype(BF16)

    def send_along(kind):
        loop(1, half, lambda o: along(kind, o).start())

    def gather_states(kind):
        cols = hcol(bit)
        loop(1, half, lambda o: along(kind, o).wait_recv())

        def both(y):
            return trow[2 * y, :, cols] + trow[2 * y + 1, :, cols]

        zero = jnp.zeros((STATE, d // 2), F32)

        def before_me(i, carry):
            total, fade = carry
            y = z - 1 - i
            total = total + jnp.exp(-fade) * lined[kind, y].astype(F32)
            return total, fade + both(y)

        def after_me(i, carry):
            total, fade = carry
            y = z + 1 + i
            total = total + jnp.exp(-fade) * lined[kind, y].astype(F32)
            return total, fade + both(y)

        none = jnp.zeros((1, d // 2), F32)
        low, _ = lax.fori_loop(0, z, before_me, (zero, none))
        high, _ = lax.fori_loop(0, half - 1 - z, after_me, (zero, none))
        lowhigh[kind, 0, :, cols] = low.astype(BF16)
        lowhigh[kind, 1, :, cols] = high.astype(BF16)

    def reach(kind):
        his = jnp.exp(-trow[twin])
        second = (bit == 1).astype(F32)
        extra = twins[kind, 1 - bit].astype(F32)
        low = lowhigh[kind, 0].astype(F32) * (1.0 - second + second * his) + extra * second
        high = lowhigh[kind, 1].astype(F32) * (second + (1.0 - second) * his) + extra * (
            1.0 - second
        )
        return low.astype(BF16), high.astype(BF16)

    def hop(up, k):
        here = ga.at[(z - k if up else z + k) * 2 + bit]
        i = 0 if up else 1
        peer = z + 1 if up else z - 1
        return at.to(here, here, s_l.at[i, k], r_l.at[i, k], sp=peer * 2 + bit)

    def came(up, k):
        here = ga.at[(z - k if up else z + k) * 2 + bit]
        i = 0 if up else 1
        return at.to(here, here, s_l.at[i, k], r_l.at[i, k - 1], sp=twin)

    def side(up, k):
        here = ga.at[(z - k if up else z + k) * 2 + bit]
        i = 0 if up else 1
        return at.to(here, here, s_ls.at[i, k], r_ls.at[i, k], sp=twin)

    def pair_gated():
        return at.to(ga.at[at.sp], ga.at[at.sp], s_x.at[0], r_x.at[0], sp=twin)

    def begin_gated():
        @pl.when(z < half - 1)
        def _():
            hop(True, 0).start()

        @pl.when(z > 0)
        def _():
            hop(False, 0).start()

        pair_gated().start()

    def advance(k):
        @pl.when(z - k >= 0)
        def _():
            came(True, k).wait_recv()

            @pl.when(z < half - 1)
            def _():
                hop(True, k).start()

            side(True, k).start()

        @pl.when(z + k < half)
        def _():
            came(False, k).wait_recv()

            @pl.when(z > 0)
            def _():
                hop(False, k).start()

            side(False, k).start()

    def place_of(i):
        return jnp.where(i < 2, i, n + 1 - i)

    def spread(k, m):
        mate = at.mate(m)
        return at.to(
            snd.at[k, mate], got.at[k, m, :, col(at.tp)], s_a2a.at[k, m], r_a2a.at[k, m], sp=mate
        )

    def share(k, m, j):
        here = got.at[k, m, :, col(at.across if j == 2 else at.tp)]
        return at.to(
            here, here, s_sh.at[k, j, m], r_sh.at[k, j, m], tp=at.across if j == 0 else at.beside
        )

    for k in (0, 1):
        loop(1, n, lambda i: spread(k, place_of(i)).start())
    for k in (0, 1):
        share(k, 0, 0).start()
        share(k, 0, 1).start()
    prepare()
    states(0, wl, vl)
    loop(1, n, lambda m: totals(m).start())
    twin_first(0).start()
    twin_rest(0).start()

    lag = 2

    def forward(q):
        k, i = lax.div(q, n), lax.rem(q, n)
        m = place_of(i)

        @pl.when(i > 0)
        def _():
            spread(k, m).wait_recv()
            share(k, m, 0).start()
            share(k, m, 1).start()

        @pl.when(q >= lag)
        def _():
            relay(q - lag)

    def relay(q):
        k, m = lax.div(q, n), place_of(lax.rem(q, n))
        share(k, m, 0).wait_recv()
        share(k, m, 2).start()

    def base_of(j):
        return jnp.where(j < 1, 0, half - j)

    def settled(k, base):
        for m in (2 * base, 2 * base + 1):
            share(k, m, 1).wait_recv()
            share(k, m, 2).wait_recv()

    def rows_of(base):
        return pl.ds(pl.multiple_of(base * duo, duo), duo)

    def ahead(j):
        base = base_of(j)
        settled(0, base)
        rows = rows_of(base)
        inputs = got[0, pl.ds(2 * base, 2)].reshape(duo, t * d)
        pg[rows, :] = dot(inputs, gate[...])
        pu[rows, :] = dot(inputs, up[...])

    def behind(j):
        base = base_of(j)
        settled(1, base)
        rows = rows_of(base)
        sent = got[1, pl.ds(2 * base, 2)].reshape(duo, t * d)
        grad = dot_last(sent, down[...])
        active, slope = silu_parts(pg[rows, :])
        ups = pu[rows, :]
        hidden[rows, :] = (active * ups).astype(BF16)
        gd[rows, :] = (grad * ups * slope).astype(BF16)
        ud[rows, :] = (grad * active).astype(BF16)

    loop(1, n, forward)
    loop(1, n, lambda m: totals(m).wait_recv())
    twin_first(0).wait_recv()
    join(0)
    for load in loads[:3]:
        load.wait()

    def second(j):
        forward(n + 2 * j)
        forward(n + 2 * j + 1)
        ahead(j)

        @pl.when(j > 0)
        def _():
            behind(j - 1)

    loop(0, half, second)
    send_along(0)
    begin_gated()
    loop(2 * n - lag, 2 * n, relay)
    behind(half - 1)

    def halves(m, k):
        c = at.cross if k == 0 else at.beside
        return at.to(
            part.at[m, :, col(c)], pair.at[k, m], s_p.at[k, m], r_p.at[k, m], tp=at.beside
        )

    def over(m):
        return at.to(summed.at[m], other.at[m], s_y.at[m], r_y.at[m], tp=at.across)

    def back(m):
        return at.to(final.at[m], arr.at[at.sp], s_b.at[m], r_b.at[m], sp=at.mate(m))

    def produce(jj):
        base = half - 1 - jj
        rows = rows_of(base)
        for c in range(t):
            cols = slice(c * d, (c + 1) * d)
            value = dot_last(gd[rows, :], gate[cols, :]) + dot_last(ud[rows, :], up[cols, :])
            part[pl.ds(2 * base, 2), :, cols] = value.astype(BF16).reshape(2, cap, d)
        for m in (2 * base + 1, 2 * base):
            for k in (0, 1):
                halves(m, k).start()

    def pass_over(jj):
        base = half - 1 - jj
        for m in (2 * base + 1, 2 * base):
            halves(m, 0).wait_recv()
            summed[m] = (
                part[m, :, col(at.across)].astype(F32) + pair[0, m].astype(F32)
            ).astype(BF16)
            over(m).start()

    def total(jj):
        base = half - 1 - jj
        for m in (2 * base + 1, 2 * base):
            halves(m, 1).wait_recv()
            over(m).wait_recv()
            final[m] = (
                part[m, :, col(at.tp)].astype(F32) + pair[1, m].astype(F32) + other[m].astype(F32)
            ).astype(BF16)

            @pl.when(m > 0)
            def _():
                back(m).start()

    def first_turn(jj):
        produce(jj)

        @pl.when(jj > 0)
        def _():
            pass_over(jj - 1)

    def weight_grads(c):
        cols = pl.ds(pl.multiple_of(c * d, d), d)
        inputs = got[0, :, :, cols].reshape(slots, d)
        gate_grad[cols, :] = dot_first(inputs, gd[...]).astype(BF16)
        up_grad[cols, :] = dot_first(inputs, ud[...]).astype(BF16)
        sent = got[1, :, :, cols].reshape(slots, d)
        down_grad[:, cols] = dot_first(hidden[...], sent).astype(BF16)

    loop(0, half, first_turn)
    pass_over(half - 1)

    def last_turn(jj):
        total(jj)

        @pl.when(jj < t)
        def _():
            weight_grads(jj)

        @pl.when(jj + 1 < half)
        def _():
            advance(jj + 1)

    loop(0, half, last_turn)
    for c in range(half, t):
        weight_grads(c)
    stores = [
        pltpu.make_async_copy(src, dst.at[0], o_sem.at[i])
        for i, (src, dst) in enumerate(
            ((gate_grad, gate_out), (up_grad, up_out), (down_grad, down_out))
        )
    ]
    for store in stores:
        store.start()
    gather_states(0)
    twin_last(0).start()
    arr[at.sp] = final[0]
    loop(1, n, lambda i: back(n - i).wait_recv())

    moe_grad = dot(pick[...], arr[...].reshape(slots, d))
    full[:, col(at.tp)] = (c_ref[...].astype(F32) + moe_grad).astype(BF16)

    def rows_to(j):
        here = full.at[:, col(at.across if j == 2 else at.tp)]
        return at.to(here, here, s_r.at[j], r_r.at[j], tp=at.across if j == 0 else at.beside)

    rows_to(0).start()
    rows_to(1).start()
    loads[3].wait()
    twin_last(0).wait_recv()
    twin_rest(0).wait_recv()
    rows_to(0).wait_recv()
    rows_to(2).start()
    rows_to(1).wait_recv()
    rows_to(2).wait_recv()

    q = tokens // t
    width = gall.shape[2]
    row = lambda tp: pl.ds(pl.multiple_of(tp * q, q), q)
    quarter = full[row(at.tp), :]
    for o in range(n):
        by[o] = quarter[:, o * width : (o + 1) * width]

    def spread_g(m):
        mate = at.mate(m)
        return at.to(
            by.at[mate], gall.at[at.sp, row(at.tp), :], s_g.at[m], r_g.at[m], sp=mate
        )

    def share_g(m, j):
        here = gall.at[at.mate(m), row(at.across if j == 2 else at.tp), :]
        return at.to(
            here, here, s_gs.at[j, m], r_gs.at[j, m], tp=at.across if j == 0 else at.beside
        )

    gall[at.sp, row(at.tp), :] = by[at.sp]
    out_delta = dot(full[...], pw[...]).astype(BF16).astype(F32)
    loop(1, n, lambda i: spread_g(place_of(i)).start())
    share_g(0, 0).start()
    share_g(0, 1).start()
    active_gate, slope_gate = silu_parts(og[...].astype(F32))
    delta[...] = (out_delta * active_gate).astype(BF16)
    states(1, rl, delta)
    twin_first(1).start()
    twin_rest(1).start()
    outg[...] = (out_delta * ms[...].astype(F32) * slope_gate).astype(BF16)

    arow = exact(rates[...], (row_id <= col_id).astype(F32))
    inner = []
    scores = []
    for g in range(groups):
        wide = slice(g * STATE, (g + 1) * STATE)
        common = dot_last(wl[:, wide], rl[:, wide])
        score = jnp.zeros((tokens, tokens), F32)
        for h in range(g * per, (g + 1) * per):
            cols = slice(h * HEAD_DIM, (h + 1) * HEAD_DIM)
            fade = jnp.exp(
                -jnp.abs(acol[:, h * HEAD_DIM : h * HEAD_DIM + 1] - arow[h : h + 1, :])
            )
            inner.append(dot((fade * common).astype(BF16), delta[:, cols]))
            score += fade * dot_last(vl[:, cols], delta[:, cols])
        scores.append(score.astype(BF16))

    twin_first(1).wait_recv()
    join(1)
    send_along(1)

    def forward_g(i):
        m = place_of(i)
        spread_g(m).wait_recv()
        share_g(m, 0).start()
        share_g(m, 1).start()

    loop(1, n, forward_g)
    a = acol[...]
    to_end = jnp.exp(a - a[tokens - 1 : tokens, :])
    to_start = jnp.exp(-a)
    w_low, w_high = reach(0)
    value = vl[...].astype(F32)
    moved = delta[...].astype(F32)
    d_start, d_end = (moved * to_start).astype(BF16), (moved * to_end).astype(BF16)
    v_start, v_end = (value * to_start).astype(BF16), (value * to_end).astype(BF16)
    for g in range(groups):
        wide = slice(g * STATE, (g + 1) * STATE)
        cols = slice(g * span, (g + 1) * span)
        rg[:, wide] = (
            dot_first(scores[g], wl[:, wide])
            + dot_last(d_start[:, cols], w_low[:, cols])
            + dot_last(d_end[:, cols], w_high[:, cols])
        ).astype(BF16)

    def relay_g(i):
        m = jnp.where(i < 1, 0, place_of(i))
        share_g(m, 0).wait_recv()
        share_g(m, 2).start()

    loop(0, n, relay_g)
    gather_states(1)
    twin_last(1).start()

    def settle_g(m):
        share_g(m, 1).wait_recv()
        share_g(m, 2).wait_recv()

    loop(0, n, settle_g)
    pair_gated().wait_recv()

    def settle_gated(k):
        @pl.when(z - k >= 0)
        def _():
            side(True, k).wait_recv()

        @pl.when(z + k < half)
        def _():
            side(False, k).wait_recv()

    loop(1, half, settle_gated)
    proj[...] = dot_first(
        gall[...].reshape(n * tokens, width), ga[...].reshape(n * tokens, d)
    )
    twin_rest(1).wait_recv()
    twin_last(1).wait_recv()
    r_low, r_high = reach(1)
    for g in range(groups):
        wide = slice(g * STATE, (g + 1) * STATE)
        cols = slice(g * span, (g + 1) * span)
        wg[:, wide] = (
            dot(scores[g], rl[:, wide])
            + dot_last(v_start[:, cols], r_low[:, cols])
            + dot_last(v_end[:, cols], r_high[:, cols])
        ).astype(BF16)
        vg[:, cols] = (
            jnp.concatenate(inner[g * per : (g + 1) * per], axis=1)
            + dot(wl[:, wide], r_low[:, cols]) * to_start[:, cols]
            + dot(wl[:, wide], r_high[:, cols]) * to_end[:, cols]
        ).astype(BF16)

    def finish(m):
        for k in (0, 1):
            for j in (0, 1, 2):
                share(k, m, j).wait_send()
            halves(m, k).wait_send()
        over(m).wait_send()
        for j in (0, 1, 2):
            share_g(m, j).wait_send()

    loop(0, n, finish)

    def finish_sp(m):
        for k in (0, 1):
            spread(k, m).wait_send()
        back(m).wait_send()
        totals(m).wait_send()
        spread_g(m).wait_send()

    loop(1, n, finish_sp)
    for j in (0, 1, 2):
        rows_to(j).wait_send()
    for kind in (0, 1):
        twin_first(kind).wait_send()
        twin_rest(kind).wait_send()
        twin_last(kind).wait_send()
        loop(1, half, lambda o: along(kind, o).wait_send())
    pair_gated().wait_send()

    def drain(k):
        @pl.when(jnp.logical_and(z - k >= 0, z < half - 1))
        def _():
            hop(True, k).wait_send()

        @pl.when(jnp.logical_and(z + k < half, z > 0))
        def _():
            hop(False, k).wait_send()

    loop(0, half, drain)

    def drain_sides(k):
        @pl.when(z - k >= 0)
        def _():
            side(True, k).wait_send()

        @pl.when(z + k < half)
        def _():
            side(False, k).wait_send()

    loop(1, half, drain_sides)
    for store in stores:
        store.wait()


def on_device(
    layer_input,
    cotangent,
    routes,
    route_weight,
    gate_weight,
    up_weight,
    down_weight,
    heads_value,
    output_gate,
    mixer_saved,
    proj_weight,
    state_write,
    state_read,
    decay_rate,
):
    n = lax.axis_size("sp")
    t = lax.axis_size("tp")
    tokens, d = layer_input.shape
    top = routes.shape[1]
    capacity = -(-max(2, 3 * tokens * top // (2 * n)) // 16) * 16
    slots = n * capacity
    hid = gate_weight.shape[2]
    half = n // 2
    width = t * d // n
    state_w = state_write.shape[1]
    sds = jax.ShapeDtypeStruct
    block = (n, capacity, d)
    vm = pl.BlockSpec(memory_space=pltpu.VMEM)
    hbm = pl.BlockSpec(memory_space=pl.ANY)
    sems = [
        (4,), (3,), (2, n), (2, n), (2, 3, n), (2, 3, n), (n,), (n,), (2, n), (2, n), (n,), (n,),
        (n,), (n,), (3,), (3,),
        (2,), (2,), (2,), (2,), (2,), (2,), (2, half), (2, half), (2, half), (2, half),
        (2, half), (2, half), (1,), (1,), (n,), (n,), (3, n), (3, n),
    ]
    return pl.pallas_call(
        functools.partial(layer_kernel, n, t, capacity),
        out_shape=(
            sds((1, t * d, hid), BF16),
            sds((1, t * d, hid), BF16),
            sds((1, hid, t * d), BF16),
            sds((width, d), F32),
            sds((tokens, d), BF16),
            sds((tokens, state_w), BF16),
            sds((tokens, state_w), BF16),
            sds((tokens, d), BF16),
        ),
        in_specs=[vm] * 10 + [hbm] * 4,
        out_specs=(hbm,) * 3 + (vm,) * 5,
        scratch_shapes=[
            VMEM((2,) + block, BF16),
            VMEM((2, n, capacity, t * d), BF16),
            VMEM((t * d, hid), BF16),
            VMEM((t * d, hid), BF16),
            VMEM((hid, t * d), BF16),
            VMEM((t * d, d), BF16),
            VMEM((slots, hid), F32),
            VMEM((slots, hid), F32),
            VMEM((slots, hid), BF16),
            VMEM((slots, hid), BF16),
            VMEM((slots, hid), BF16),
            VMEM((n, capacity, t * d), BF16),
            VMEM((2,) + block, BF16),
            VMEM(block, BF16),
            VMEM(block, BF16),
            VMEM(block, BF16),
            VMEM(block, BF16),
            VMEM((tokens, slots), BF16),
            VMEM((t * d, hid), BF16),
            VMEM((t * d, hid), BF16),
            VMEM((hid, t * d), BF16),
            VMEM((n, 1, d), F32),
            VMEM((tokens, d), F32),
            VMEM((2, 2, STATE, d), BF16),
            VMEM((2, 2, STATE, d), BF16),
            VMEM((2, 2, STATE, d // 2), BF16),
            VMEM((2, half, STATE, d // 2), BF16),
            VMEM((2, 2, STATE, d), BF16),
            VMEM((tokens, d), BF16),
            VMEM((n, tokens, d), BF16),
            VMEM((tokens, t * d), BF16),
            VMEM((n, tokens // t, width), BF16),
            VMEM((n, tokens, width), BF16),
        ] + [DMA(shape) for shape in sems],
        compiler_params=pltpu.CompilerParams(
            collective_id=1,
            has_side_effects=True,
            vmem_limit_bytes=60 * 1024 * 1024,
        ),
        cost_estimate=pl.CostEstimate(
            flops=4_000_000_000, bytes_accessed=8_000_000, transcendentals=0
        ),
        name="layer",
    )(
        routes.T,
        route_weight.T,
        decay_rate.T,
        layer_input,
        cotangent,
        heads_value,
        output_gate,
        mixer_saved,
        state_write,
        state_read,
        gate_weight,
        up_weight,
        down_weight,
        proj_weight,
    )


def solution(mesh):
    split = P("sp", "tp")
    in_specs = (
        split,
        split,
        P("sp", None),
        P("sp", None),
        P("sp", None, "tp"),
        P("sp", None, "tp"),
        P("sp", "tp", None),
        split,
        split,
        split,
        P(None, "tp"),
        split,
        split,
        split,
    )
    out_specs = (
        P("sp", None, "tp"),
        P("sp", None, "tp"),
        P("sp", "tp", None),
        split,
        split,
        split,
        split,
        split,
    )
    return jax.shard_map(
        on_device, mesh=mesh, in_specs=in_specs, out_specs=out_specs, check_vma=False
    )
```

time: 145 us -> 102 us (0.70)
  Pallas kernels: 130 us -> 93.7 us
  matrix products: 3.59 us -> 0 us
  local copies, waits for them, and re-layouts: 9.4 us -> 7.71 us
    pallas_call x3 -> x1, Pallas kernels: 130 us -> 93.7 us  [on_device(): pl.pallas_call(functools.partial(layer_kernel, n, t, capacity), out_shape...]
    dot_general x2 -> x0, matrix products: 3.59 us -> none  [the longest x1 2.34 us: on_device(): jnp.dot(full_grad, proj_weight, preferred_element_type=F32).astype(BF16)]
    unnamed x26 -> x22, local copies, waits for them, and re-layouts: 6.71 us -> 7.71 us
where the time goes in v2:
time: 102 us
  Pallas kernels  93.7 us (92%)
  local copies, waits for them, and re-layouts  7.71 us (8%)
    pallas_call x1, Pallas kernels, on_device(): pl.pallas_call(functools.partial(layer_kernel, n, t, capacity), out_shape...  93.7 us
    unnamed x22, local copies, waits for them, and re-layouts  7.71 us

profile of v2, /device:TPU:0, one launch (start us, length us, event | category | flops | bytes accessed | tf_op | source)
XLA Modules:
  0.0 102.1 jit_solution(15606121440460909489)
XLA Ops:
  0.6 93.7 %layer.1 = (bf16[1,2048,256]{2,1,0:T(8,128)(2,1)}, bf16[1,2048,256]{2,1,0:T(8,128)(2,1)}, bf16[1,256,2048]{2,1,0:T(8,128)(2,1)}, f32[256,512]{1,0:T(8,128)}, bf1...) custom-call(s32[2,128]{1,0:T(2,128)} %bitcast.4, ...), custom_call_target="tpu_custom_call" | custom-call | flops 4000000000 | bytes 8000000 | tf_op jit(solution)/shard_map/layer/pallas_call | solution.py:729
  94.3 0.0 copy-start.1
  94.3 0.0 copy-start
  94.3 2.4 %copy.30 = bf16[1,2048,256]{2,1,0:T(8,128)(2,1)} copy(bf16[1,2048,256]{2,1,0:T(8,128)(2,1)} %get-tuple-element.16) | data formatting | bytes 2097152
  96.7 0.0 copy-done.1
  96.7 0.0 copy-start.2
  96.7 1.0 copy.31
  97.7 0.0 copy-done
  97.7 0.0 copy-start.4
  97.7 0.0 copy-start.6
  97.7 0.0 copy-start.5
  97.7 0.0 copy-start.3
  97.7 1.0 copy.32
  98.7 0.0 copy-done.2
  98.7 0.8 copy.33
  99.5 0.0 copy-done.4
  99.5 0.7 copy.34
  100.2 0.0 copy-done.6
  100.2 0.6 copy.35
  100.8 0.0 copy-done.5
  100.8 0.6 copy.36
  101.4 0.0 copy-done.3
  101.4 0.7 copy.37
Async XLA Ops:
  94.3 2.4 %copy-start.1 = (bf16[1,2048,256]{2,1,0:T(8,128)(2,1)S(1)}, bf16[1,2048,256]{2,1,0:T(8,128)(2,1)}, u32[]{:S(2)}) copy-start(bf16[1,2048,256]{2,1,0:T(8,128)(2,1)} %get-tuple-element.17) | copy-start | bytes 3145732
  94.3 3.4 %copy-start = (bf16[1,256,2048]{2,1,0:T(8,128)(2,1)S(1)}, bf16[1,256,2048]{2,1,0:T(8,128)(2,1)}, u32[]{:S(2)}) copy-start(bf16[1,256,2048]{2,1,0:T(8,128)(2,1)} %get-tuple-element.18) | copy-start | bytes 3145732
  96.7 2.0 %copy-start.2 = (f32[256,512]{1,0:T(8,128)S(1)}, f32[256,512]{1,0:T(8,128)}, u32[]{:S(2)}) copy-start(f32[256,512]{1,0:T(8,128)} %get-tuple-element.19) | copy-start | bytes 1572868
  97.7 1.8 %copy-start.4 = (bf16[128,512]{1,0:T(8,128)(2,1)S(1)}, bf16[128,512]{1,0:T(8,128)(2,1)}, u32[]{:S(2)}) copy-start(bf16[128,512]{1,0:T(8,128)(2,1)} %get-tuple-element.20) | copy-start | bytes 393220
  97.7 2.4 %copy-start.6 = (bf16[128,128]{1,0:T(8,128)(2,1)S(1)}, bf16[128,128]{1,0:T(8,128)(2,1)}, u32[]{:S(2)}) copy-start(bf16[128,128]{1,0:T(8,128)(2,1)} %get-tuple-element.21) | copy-start | bytes 98308
  97.7 3.1 %copy-start.5 = (bf16[128,128]{1,0:T(8,128)(2,1)S(1)}, bf16[128,128]{1,0:T(8,128)(2,1)}, u32[]{:S(2)}) copy-start(bf16[128,128]{1,0:T(8,128)(2,1)} %get-tuple-element.22) | copy-start | bytes 98308
  97.7 3.7 %copy-start.3 = (bf16[128,512]{1,0:T(8,128)(2,1)S(1)}, bf16[128,512]{1,0:T(8,128)(2,1)}, u32[]{:S(2)}) copy-start(bf16[128,512]{1,0:T(8,128)(2,1)} %get-tuple-element.23) | copy-start | bytes 393220

commit v3 on v2

--- a/solution.py
+++ b/solution.py
@@ -16,6 +16,7 @@
 BF16 = jnp.bfloat16
 VMEM = pltpu.VMEM
 DMA = pltpu.SemaphoreType.DMA
+MIB = 1024 * 1024
 
 
 def silu_parts(value):
@@ -83,11 +84,11 @@
 def layer_kernel(
     n, t, cap,
     routes, rweight, rates, x_ref, c_ref, vl, og, ms, wl, rl, gate_hbm, up_hbm, down_hbm, pw_hbm,
-    gate_out, up_out, down_out, proj, vg, wg, rg, outg,
+    gate_grad, up_grad, down_grad, proj, vg, wg, rg, outg,
     snd, got, gate, up, down, pw, pg, pu, hidden, gd, ud, part, pair, summed, other, final, arr,
-    pick, gate_grad, up_grad, down_grad, trow, acol, ends, twins, joint, lined, lowhigh, delta,
+    pick, trow, acol, ends, twins, joint, lined, lowhigh, delta,
     ga, full, by, gall,
-    w_sem, o_sem, s_a2a, r_a2a, s_sh, r_sh, s_d, r_d, s_p, r_p, s_y, r_y, s_b, r_b, s_r, r_r,
+    w_sem, s_a2a, r_a2a, s_sh, r_sh, s_d, r_d, s_p, r_p, s_y, r_y, s_b, r_b, s_r, r_r,
     s_t1, r_t1, s_t2, r_t2, s_t3, r_t3, s_z, r_z, s_l, r_l, s_ls, r_ls, s_x, r_x, s_g, r_g,
     s_gs, r_gs,
 ):
@@ -309,9 +310,6 @@
 
             side(False, k).start()
 
-    def place_of(i):
-        return jnp.where(i < 2, i, n + 1 - i)
-
     def spread(k, m):
         mate = at.mate(m)
         return at.to(
@@ -325,7 +323,7 @@
         )
 
     for k in (0, 1):
-        loop(1, n, lambda i: spread(k, place_of(i)).start())
+        loop(1, n, lambda i: spread(k, i).start())
     for k in (0, 1):
         share(k, 0, 0).start()
         share(k, 0, 1).start()
@@ -339,7 +337,7 @@
 
     def forward(q):
         k, i = lax.div(q, n), lax.rem(q, n)
-        m = place_of(i)
+        m = i
 
         @pl.when(i > 0)
         def _():
@@ -352,12 +350,9 @@
             relay(q - lag)
 
     def relay(q):
-        k, m = lax.div(q, n), place_of(lax.rem(q, n))
+        k, m = lax.div(q, n), lax.rem(q, n)
         share(k, m, 0).wait_recv()
         share(k, m, 2).start()
-
-    def base_of(j):
-        return jnp.where(j < 1, 0, half - j)
 
     def settled(k, base):
         for m in (2 * base, 2 * base + 1):
@@ -368,7 +363,7 @@
         return pl.ds(pl.multiple_of(base * duo, duo), duo)
 
     def ahead(j):
-        base = base_of(j)
+        base = j
         settled(0, base)
         rows = rows_of(base)
         inputs = got[0, pl.ds(2 * base, 2)].reshape(duo, t * d)
@@ -376,7 +371,7 @@
         pu[rows, :] = dot(inputs, up[...])
 
     def behind(j):
-        base = base_of(j)
+        base = j
         settled(1, base)
         rows = rows_of(base)
         sent = got[1, pl.ds(2 * base, 2)].reshape(duo, t * d)
@@ -388,9 +383,6 @@
         ud[rows, :] = (grad * active).astype(BF16)
 
     loop(1, n, forward)
-    loop(1, n, lambda m: totals(m).wait_recv())
-    twin_first(0).wait_recv()
-    join(0)
     for load in loads[:3]:
         load.wait()
 
@@ -404,7 +396,6 @@
             behind(j - 1)
 
     loop(0, half, second)
-    send_along(0)
     begin_gated()
     loop(2 * n - lag, 2 * n, relay)
     behind(half - 1)
@@ -464,13 +455,15 @@
     def weight_grads(c):
         cols = pl.ds(pl.multiple_of(c * d, d), d)
         inputs = got[0, :, :, cols].reshape(slots, d)
-        gate_grad[cols, :] = dot_first(inputs, gd[...]).astype(BF16)
-        up_grad[cols, :] = dot_first(inputs, ud[...]).astype(BF16)
+        gate_grad[0, cols, :] = dot_first(inputs, gd[...]).astype(BF16)
+        up_grad[0, cols, :] = dot_first(inputs, ud[...]).astype(BF16)
         sent = got[1, :, :, cols].reshape(slots, d)
-        down_grad[:, cols] = dot_first(hidden[...], sent).astype(BF16)
+        down_grad[0, :, cols] = dot_first(hidden[...], sent).astype(BF16)
 
     loop(0, half, first_turn)
     pass_over(half - 1)
+    if half > 1:
+        advance(1)
 
     def last_turn(jj):
         total(jj)
@@ -478,24 +471,16 @@
         @pl.when(jj < t)
         def _():
             weight_grads(jj)
-
-        @pl.when(jj + 1 < half)
-        def _():
-            advance(jj + 1)
 
     loop(0, half, last_turn)
     for c in range(half, t):
         weight_grads(c)
-    stores = [
-        pltpu.make_async_copy(src, dst.at[0], o_sem.at[i])
-        for i, (src, dst) in enumerate(
-            ((gate_grad, gate_out), (up_grad, up_out), (down_grad, down_out))
-        )
-    ]
-    for store in stores:
-        store.start()
-    gather_states(0)
-    twin_last(0).start()
+    loop(1, n, lambda m: totals(m).wait_recv())
+    twin_first(0).wait_recv()
+    join(0)
+    send_along(0)
+    if half > 3:
+        loop(2, half - 1, advance)
     arr[at.sp] = final[0]
     loop(1, n, lambda i: back(n - i).wait_recv())
 
@@ -509,10 +494,10 @@
     rows_to(0).start()
     rows_to(1).start()
     loads[3].wait()
-    twin_last(0).wait_recv()
-    twin_rest(0).wait_recv()
     rows_to(0).wait_recv()
     rows_to(2).start()
+    if half > 2:
+        advance(half - 1)
     rows_to(1).wait_recv()
     rows_to(2).wait_recv()
 
@@ -537,7 +522,7 @@
 
     gall[at.sp, row(at.tp), :] = by[at.sp]
     out_delta = dot(full[...], pw[...]).astype(BF16).astype(F32)
-    loop(1, n, lambda i: spread_g(place_of(i)).start())
+    loop(1, n, lambda i: spread_g(i).start())
     share_g(0, 0).start()
     share_g(0, 1).start()
     active_gate, slope_gate = silu_parts(og[...].astype(F32))
@@ -566,14 +551,45 @@
     twin_first(1).wait_recv()
     join(1)
     send_along(1)
-
-    def forward_g(i):
-        m = place_of(i)
+    gather_states(0)
+    twin_last(0).start()
+
+    def forward_g(m):
         spread_g(m).wait_recv()
         share_g(m, 0).start()
         share_g(m, 1).start()
 
     loop(1, n, forward_g)
+    def relay_g(m):
+        share_g(m, 0).wait_recv()
+        share_g(m, 2).start()
+
+    loop(0, n, relay_g)
+    gather_states(1)
+    twin_last(1).start()
+
+    def settle_g(m):
+        share_g(m, 1).wait_recv()
+        share_g(m, 2).wait_recv()
+
+    loop(0, n, settle_g)
+    pair_gated().wait_recv()
+
+    def settle_gated(k):
+        @pl.when(z - k >= 0)
+        def _():
+            side(True, k).wait_recv()
+
+        @pl.when(z + k < half)
+        def _():
+            side(False, k).wait_recv()
+
+    loop(1, half, settle_gated)
+    proj[...] = dot_first(
+        gall[...].reshape(n * tokens, width), ga[...].reshape(n * tokens, d)
+    )
+    twin_rest(0).wait_recv()
+    twin_last(0).wait_recv()
     a = acol[...]
     to_end = jnp.exp(a - a[tokens - 1 : tokens, :])
     to_start = jnp.exp(-a)
@@ -591,35 +607,6 @@
             + dot_last(d_end[:, cols], w_high[:, cols])
         ).astype(BF16)
 
-    def relay_g(i):
-        m = jnp.where(i < 1, 0, place_of(i))
-        share_g(m, 0).wait_recv()
-        share_g(m, 2).start()
-
-    loop(0, n, relay_g)
-    gather_states(1)
-    twin_last(1).start()
-
-    def settle_g(m):
-        share_g(m, 1).wait_recv()
-        share_g(m, 2).wait_recv()
-
-    loop(0, n, settle_g)
-    pair_gated().wait_recv()
-
-    def settle_gated(k):
-        @pl.when(z - k >= 0)
-        def _():
-            side(True, k).wait_recv()
-
-        @pl.when(z + k < half)
-        def _():
-            side(False, k).wait_recv()
-
-    loop(1, half, settle_gated)
-    proj[...] = dot_first(
-        gall[...].reshape(n * tokens, width), ga[...].reshape(n * tokens, d)
-    )
     twin_rest(1).wait_recv()
     twin_last(1).wait_recv()
     r_low, r_high = reach(1)
@@ -686,8 +673,24 @@
             side(False, k).wait_send()
 
     loop(1, half, drain_sides)
-    for store in stores:
-        store.wait()
+
+
+def put_out_kernel(*refs):
+    count = len(refs) // 2
+    copies = [
+        pltpu.make_async_copy(refs[i], refs[count + i], refs[-1].at[i]) for i in range(count)
+    ]
+    for copy in copies:
+        copy.start()
+    for copy in copies:
+        copy.wait()
+
+
+def held(scratch):
+    shape, size = scratch.shape, jnp.dtype(scratch.dtype).itemsize
+    minor = -(-shape[-1] // 128) * 128
+    rows = -(-shape[-2] // 16) * 16
+    return functools.reduce(lambda a, b: a * b, shape[:-2], minor * rows * size)
 
 
 def on_device(
@@ -719,66 +722,65 @@
     sds = jax.ShapeDtypeStruct
     block = (n, capacity, d)
     vm = pl.BlockSpec(memory_space=pltpu.VMEM)
-    hbm = pl.BlockSpec(memory_space=pl.ANY)
+    hbm = pl.BlockSpec(memory_space=pltpu.HBM)
     sems = [
-        (4,), (3,), (2, n), (2, n), (2, 3, n), (2, 3, n), (n,), (n,), (2, n), (2, n), (n,), (n,),
+        (4,), (2, n), (2, n), (2, 3, n), (2, 3, n), (n,), (n,), (2, n), (2, n), (n,), (n,),
         (n,), (n,), (3,), (3,),
         (2,), (2,), (2,), (2,), (2,), (2,), (2, half), (2, half), (2, half), (2, half),
         (2, half), (2, half), (1,), (1,), (n,), (n,), (3, n), (3, n),
     ]
-    return pl.pallas_call(
+    outs = (
+        sds((1, t * d, hid), BF16),
+        sds((1, t * d, hid), BF16),
+        sds((1, hid, t * d), BF16),
+        sds((width, d), F32),
+        sds((tokens, d), BF16),
+        sds((tokens, state_w), BF16),
+        sds((tokens, state_w), BF16),
+        sds((tokens, d), BF16),
+    )
+    scratch = [
+        VMEM((2,) + block, BF16),
+        VMEM((2, n, capacity, t * d), BF16),
+        VMEM((t * d, hid), BF16),
+        VMEM((t * d, hid), BF16),
+        VMEM((hid, t * d), BF16),
+        VMEM((t * d, d), BF16),
+        VMEM((slots, hid), F32),
+        VMEM((slots, hid), F32),
+        VMEM((slots, hid), BF16),
+        VMEM((slots, hid), BF16),
+        VMEM((slots, hid), BF16),
+        VMEM((n, capacity, t * d), BF16),
+        VMEM((2,) + block, BF16),
+        VMEM(block, BF16),
+        VMEM(block, BF16),
+        VMEM(block, BF16),
+        VMEM(block, BF16),
+        VMEM((tokens, slots), BF16),
+        VMEM((n, 1, d), F32),
+        VMEM((tokens, d), F32),
+        VMEM((2, 2, STATE, d), BF16),
+        VMEM((2, 2, STATE, d), BF16),
+        VMEM((2, 2, STATE, d // 2), BF16),
+        VMEM((2, half, STATE, d // 2), BF16),
+        VMEM((2, 2, STATE, d), BF16),
+        VMEM((tokens, d), BF16),
+        VMEM((n, tokens, d), BF16),
+        VMEM((tokens, t * d), BF16),
+        VMEM((n, tokens // t, width), BF16),
+        VMEM((n, tokens, width), BF16),
+    ]
+    grads = pl.pallas_call(
         functools.partial(layer_kernel, n, t, capacity),
-        out_shape=(
-            sds((1, t * d, hid), BF16),
-            sds((1, t * d, hid), BF16),
-            sds((1, hid, t * d), BF16),
-            sds((width, d), F32),
-            sds((tokens, d), BF16),
-            sds((tokens, state_w), BF16),
-            sds((tokens, state_w), BF16),
-            sds((tokens, d), BF16),
-        ),
+        out_shape=outs,
         in_specs=[vm] * 10 + [hbm] * 4,
-        out_specs=(hbm,) * 3 + (vm,) * 5,
-        scratch_shapes=[
-            VMEM((2,) + block, BF16),
-            VMEM((2, n, capacity, t * d), BF16),
-            VMEM((t * d, hid), BF16),
-            VMEM((t * d, hid), BF16),
-            VMEM((hid, t * d), BF16),
-            VMEM((t * d, d), BF16),
-            VMEM((slots, hid), F32),
-            VMEM((slots, hid), F32),
-            VMEM((slots, hid), BF16),
-            VMEM((slots, hid), BF16),
-            VMEM((slots, hid), BF16),
-            VMEM((n, capacity, t * d), BF16),
-            VMEM((2,) + block, BF16),
-            VMEM(block, BF16),
-            VMEM(block, BF16),
-            VMEM(block, BF16),
-            VMEM(block, BF16),
-            VMEM((tokens, slots), BF16),
-            VMEM((t * d, hid), BF16),
-            VMEM((t * d, hid), BF16),
-            VMEM((hid, t * d), BF16),
-            VMEM((n, 1, d), F32),
-            VMEM((tokens, d), F32),
-            VMEM((2, 2, STATE, d), BF16),
-            VMEM((2, 2, STATE, d), BF16),
-            VMEM((2, 2, STATE, d // 2), BF16),
-            VMEM((2, half, STATE, d // 2), BF16),
-            VMEM((2, 2, STATE, d), BF16),
-            VMEM((tokens, d), BF16),
-            VMEM((n, tokens, d), BF16),
-            VMEM((tokens, t * d), BF16),
-            VMEM((n, tokens // t, width), BF16),
-            VMEM((n, tokens, width), BF16),
-        ] + [DMA(shape) for shape in sems],
+        out_specs=(vm,) * 8,
+        scratch_shapes=scratch + [DMA(shape) for shape in sems],
         compiler_params=pltpu.CompilerParams(
             collective_id=1,
             has_side_effects=True,
-            vmem_limit_bytes=60 * 1024 * 1024,
+            vmem_limit_bytes=min(60 * MIB, sum(map(held, scratch)) + 8 * MIB),
         ),
         cost_estimate=pl.CostEstimate(
             flops=4_000_000_000, bytes_accessed=8_000_000, transcendentals=0
@@ -800,6 +802,15 @@
         down_weight,
         proj_weight,
     )
+    return pl.pallas_call(
+        put_out_kernel,
+        out_shape=outs,
+        in_specs=[vm] * len(outs),
+        out_specs=(hbm,) * len(outs),
+        scratch_shapes=[DMA((len(outs),))],
+        compiler_params=pltpu.CompilerParams(vmem_limit_bytes=12 * MIB),
+        name="put_out",
+    )(*grads)
 
 
 def solution(mesh):

time: 102 us -> 97.3 us (0.954)
  Pallas kernels: 93.7 us -> 82.7 us
  local copies, waits for them, and re-layouts: 7.71 us -> 13.3 us
    pallas_call x1, Pallas kernels: 93.7 us -> 80.7 us  [on_device(): pl.pallas_call(functools.partial(layer_kernel, n, t, capacity), out_shape...]
    unnamed x22 -> x28, local copies, waits for them, and re-layouts: 7.71 us -> 13.3 us
    pallas_call x0 -> x1, Pallas kernels: none -> 2 us  [on_device(): pl.pallas_call(put_out_kernel, out_shape=outs, in_specs=[vm] * len(outs),...]
where the time goes in v3:
time: 97.3 us; the launch traced here: 96.7 us
  Pallas kernels  82.7 us (85%)
  local copies, waits for them, and re-layouts  13.3 us (14%)
    pallas_call x1, Pallas kernels, on_device(): pl.pallas_call(functools.partial(layer_kernel, n, t, capacity), out_shape...  80.7 us
    unnamed x28, local copies, waits for them, and re-layouts  13.3 us
    pallas_call x1, Pallas kernels, on_device(): pl.pallas_call(put_out_kernel, out_shape=outs, in_specs=[vm] * len(outs),...  2 us

profile of v3, /device:TPU:0, one launch (start us, length us, event | category | flops | bytes accessed | tf_op | source)
XLA Modules:
  0.0 96.7 jit_solution(14240404595073872300)
XLA Ops:
  0.6 0.0 copy-start
  0.6 1.6 %copy-done = bf16[2048,512]{1,0:T(8,128)(2,1)S(1)} copy-done((bf16[2048,512]{1,0:T(8,128)(2,1)S(1)}, bf16[2048,512]{1,0:T(8,128)(2,1)}, u32[]{:S(2)}) %copy-start) | copy-done | bytes 2097176
  2.2 0.0 copy-start.1
  2.2 1.2 %copy-done.1 = bf16[1,2048,256]{2,1,0:T(8,128)(2,1)S(1)} copy-done((bf16[1,2048,256]{2,1,0:T(8,128)(2,1)S(1)}, bf16[1,2048,256]{2,1,0:T(8,128)(2,1)}, u32[]{:S(2)}) %copy-start.1) | copy-done | bytes 1048600
  3.5 0.0 copy-start.2
  3.5 1.2 %copy-done.2 = bf16[1,2048,256]{2,1,0:T(8,128)(2,1)S(1)} copy-done((bf16[1,2048,256]{2,1,0:T(8,128)(2,1)S(1)}, bf16[1,2048,256]{2,1,0:T(8,128)(2,1)}, u32[]{:S(2)}) %copy-start.2) | copy-done | bytes 1048600
  4.7 0.0 copy-start.3
  4.7 1.2 %copy-done.3 = bf16[1,256,2048]{2,1,0:T(8,128)(2,1)S(1)} copy-done((bf16[1,256,2048]{2,1,0:T(8,128)(2,1)S(1)}, bf16[1,256,2048]{2,1,0:T(8,128)(2,1)}, u32[]{:S(2)}) %copy-start.3) | copy-done | bytes 1048600
  5.9 0.0 copy-start.4
  5.9 0.9 copy-done.4
  6.8 0.0 copy-start.5
  6.8 0.9 copy-done.5
  7.7 0.0 copy-start.6
  7.7 0.9 copy-done.6
  8.6 0.0 copy-start.7
  8.6 0.9 copy-done.7
  9.5 0.0 copy-start.8
  9.5 0.9 copy-done.8
  10.4 0.0 copy-start.9
  10.4 0.8 copy-done.9
  11.2 0.0 copy-start.10
  11.2 0.8 copy-done.10
  11.9 0.0 copy-start.11
  11.9 0.7 copy-done.11
  12.6 0.0 copy-start.12
  12.6 0.7 copy-done.12
  13.3 0.0 copy-start.13
  13.3 0.7 copy-done.13
  14.0 80.7 %layer.1 = (bf16[1,2048,256]{2,1,0:T(8,128)(2,1)S(1)}, bf16[1,2048,256]{2,1,0:T(8,128)(2,1)S(1)}, bf16[1,256,2048]{2,1,0:T(8,128)(2,1)S(1)}, f32[256,512]{1,0:T(...) custom-call(s32[2,128]{1,0:T(2,128)S(1)} %bitcast.4, ...), custom_call_target="tpu_custom_call" | custom-call | flops 4000000000 | bytes 8000000 | tf_op jit(solution)/shard_map/layer/pallas_call | solution.py:774
  94.7 2.0 %put_out.1 = (bf16[1,2048,256]{2,1,0:T(8,128)(2,1)}, bf16[1,2048,256]{2,1,0:T(8,128)(2,1)}, bf16[1,256,2048]{2,1,0:T(8,128)(2,1)}, f32[256,512]{1,0:T(8,128)}, b...) custom-call(bf16[1,2048,256]{2,1,0:T(8,128)(2,1)S(1)} %get-tuple-elemen, ...), custom_call_target="tpu_custom_call" | custom-call | tf_op jit(solution)/shard_map/put_out/pallas_call | solution.py:805
Async XLA Ops:
  0.6 1.6 %copy-start = (bf16[2048,512]{1,0:T(8,128)(2,1)S(1)}, bf16[2048,512]{1,0:T(8,128)(2,1)}, u32[]{:S(2)}) copy-start(bf16[2048,512]{1,0:T(8,128)(2,1)} %pw_hbm.1) | copy-start | bytes 6291460
  2.2 1.2 %copy-start.1 = (bf16[1,2048,256]{2,1,0:T(8,128)(2,1)S(1)}, bf16[1,2048,256]{2,1,0:T(8,128)(2,1)}, u32[]{:S(2)}) copy-start(bf16[1,2048,256]{2,1,0:T(8,128)(2,1)} %gate_hbm.1) | copy-start | bytes 3145732
  3.5 1.2 %copy-start.2 = (bf16[1,2048,256]{2,1,0:T(8,128)(2,1)S(1)}, bf16[1,2048,256]{2,1,0:T(8,128)(2,1)}, u32[]{:S(2)}) copy-start(bf16[1,2048,256]{2,1,0:T(8,128)(2,1)} %up_hbm.1) | copy-start | bytes 3145732
  4.7 1.2 %copy-start.3 = (bf16[1,256,2048]{2,1,0:T(8,128)(2,1)S(1)}, bf16[1,256,2048]{2,1,0:T(8,128)(2,1)}, u32[]{:S(2)}) copy-start(bf16[1,256,2048]{2,1,0:T(8,128)(2,1)} %down_hbm.1) | copy-start | bytes 3145732
  5.9 0.9 copy-start.4
  6.8 0.9 copy-start.5
  7.7 0.9 copy-start.6
  8.6 0.9 copy-start.7
  9.5 0.9 copy-start.8
  10.4 0.8 copy-start.9
  11.2 0.8 copy-start.10
  11.9 0.7 copy-start.11
  12.6 0.7 copy-start.12
  13.3 0.7 copy-start.13

commit v4 on v3

--- a/solution.py
+++ b/solution.py
@@ -81,17 +81,21 @@
     lax.fori_loop(lo, hi, step, 0)
 
 
-def layer_kernel(
-    n, t, cap,
-    routes, rweight, rates, x_ref, c_ref, vl, og, ms, wl, rl, gate_hbm, up_hbm, down_hbm, pw_hbm,
-    gate_grad, up_grad, down_grad, proj, vg, wg, rg, outg,
-    snd, got, gate, up, down, pw, pg, pu, hidden, gd, ud, part, pair, summed, other, final, arr,
-    pick, trow, acol, ends, twins, joint, lined, lowhigh, delta,
-    ga, full, by, gall,
-    w_sem, s_a2a, r_a2a, s_sh, r_sh, s_d, r_d, s_p, r_p, s_y, r_y, s_b, r_b, s_r, r_r,
-    s_t1, r_t1, s_t2, r_t2, s_t3, r_t3, s_z, r_z, s_l, r_l, s_ls, r_ls, s_x, r_x, s_g, r_g,
-    s_gs, r_gs,
-):
+def layer_kernel(n, t, cap, *refs):
+    count = 14
+    sources, refs = refs[:count], refs[count:]
+    gate_grad, up_grad, down_grad, proj, vg, wg, rg, outg = refs[:8]
+    held_in, refs = refs[8 : 8 + count], refs[8 + count :]
+    routes, rweight, rates, x_ref, c_ref, vl, og, ms, wl, rl, gate, up, down, pw = held_in
+    (
+        snd, got, pg, pu, hidden, gd, ud, part, pair, summed, other, final, arr, pick, trow,
+        acol, fades, act, slp, ends, twins, joint, lined, lowhigh, delta, ga, full, by, gall,
+    ) = refs[:29]
+    (
+        w_sem, s_a2a, r_a2a, s_sh, r_sh, s_d, r_d, s_p, r_p, s_y, r_y, s_b, r_b, s_r, r_r,
+        s_t1, r_t1, s_t2, r_t2, s_t3, r_t3, s_z, r_z, s_l, r_l, s_ls, r_ls, s_x, r_x, s_g, r_g,
+        s_gs, r_gs,
+    ) = refs[29:]
     at = Place(n, t)
     tokens, d = x_ref.shape
     top = routes.shape[0]
@@ -108,23 +112,26 @@
     col = lambda tp: pl.ds(pl.multiple_of(tp * d, d), d)
     hcol = lambda b: pl.ds(pl.multiple_of(b * (d // 2), d // 2), d // 2)
 
-    weights_in = ((gate_hbm.at[0], gate), (up_hbm.at[0], up), (down_hbm.at[0], down), (pw_hbm, pw))
+    barrier = pltpu.get_barrier_semaphore()
+    for tp in (at.across, at.beside):
+        pl.semaphore_signal(barrier, inc=1, device_id=(at.sp, tp), device_id_type=MESH)
+
+    def hello(o):
+        pl.semaphore_signal(
+            barrier, inc=1, device_id=(lax.rem(at.sp + o, n), at.tp), device_id_type=MESH
+        )
+
+    loop(1, n, hello)
     loads = [
-        pltpu.make_async_copy(src, dst, w_sem.at[i]) for i, (src, dst) in enumerate(weights_in)
+        pltpu.make_async_copy(
+            src if len(src.shape) == len(dst.shape) else src.at[0], dst, w_sem.at[i]
+        )
+        for i, (src, dst) in enumerate(zip(sources, held_in))
     ]
     for load in loads:
         load.start()
-
-    barrier = pltpu.get_barrier_semaphore()
-    for tp in (at.across, at.beside):
-        pl.semaphore_signal(barrier, inc=1, device_id=(at.sp, tp), device_id_type=MESH)
-
-    def hello(o):
-        pl.semaphore_signal(
-            barrier, inc=1, device_id=(lax.rem(at.sp + o, n), at.tp), device_id_type=MESH
-        )
-
-    loop(1, n, hello)
+    for load in loads[:5]:
+        load.wait()
 
     row_id = lax.broadcasted_iota(jnp.int32, (tokens, tokens), 0)
     col_id = lax.broadcasted_iota(jnp.int32, (tokens, tokens), 1)
@@ -151,7 +158,6 @@
         got[k, 0, :, col(at.tp)] = snd[k, at.sp]
     pl.semaphore_wait(barrier, n + 1)
 
-
     def to_columns(value):
         lane = lax.broadcasted_iota(jnp.int32, (heads, d), 1)
         lead = lax.broadcasted_iota(jnp.int32, (heads, d), 0) * HEAD_DIM
@@ -162,15 +168,19 @@
         upto = (row_id >= col_id).astype(F32)
         acol[...] = exact(upto, to_columns(rates[...]))
         trow[at.sp] = acol[tokens - 1 : tokens, :]
-        ga[at.sp] = (
-            ms[...].astype(F32) * silu_parts(og[...].astype(F32))[0]
-        ).astype(BF16)
+        a = acol[...]
+        fades[0] = jnp.exp(a - a[tokens - 1 : tokens, :])
+        fades[1] = jnp.exp(-a)
+        active_gate, slope_gate = silu_parts(og[...].astype(F32))
+        saved = ms[...].astype(F32)
+        ga[at.sp] = (saved * active_gate).astype(BF16)
+        act[...] = active_gate
+        slp[...] = saved * slope_gate
 
     def states(kind, left, right):
-        a = acol[...]
         value = right[...].astype(F32)
-        for i, fade in enumerate((jnp.exp(a - a[tokens - 1 : tokens, :]), jnp.exp(-a))):
-            faded = (value * fade).astype(BF16)
+        for i in (0, 1):
+            faded = (value * fades[i]).astype(BF16)
             for g in range(groups):
                 ends[kind, i, :, g * span : (g + 1) * span] = dot_first(
                     left[:, g * STATE : (g + 1) * STATE], faded[:, g * span : (g + 1) * span]
@@ -287,9 +297,7 @@
         def _():
             hop(False, 0).start()
 
-        pair_gated().start()
-
-    def advance(k):
+    def pass_on(k):
         @pl.when(z - k >= 0)
         def _():
             came(True, k).wait_recv()
@@ -298,8 +306,6 @@
             def _():
                 hop(True, k).start()
 
-            side(True, k).start()
-
         @pl.when(z + k < half)
         def _():
             came(False, k).wait_recv()
@@ -308,6 +314,13 @@
             def _():
                 hop(False, k).start()
 
+    def sides(k):
+        @pl.when(z - k >= 0)
+        def _():
+            side(True, k).start()
+
+        @pl.when(z + k < half)
+        def _():
             side(False, k).start()
 
     def spread(k, m):
@@ -322,22 +335,28 @@
             here, here, s_sh.at[k, j, m], r_sh.at[k, j, m], tp=at.across if j == 0 else at.beside
         )
 
+    def place_of(k, i):
+        return jnp.where(jnp.logical_and(k == 1, i > 1), n + 1 - i, i)
+
     for k in (0, 1):
-        loop(1, n, lambda i: spread(k, i).start())
+        loop(1, n, lambda i: spread(k, place_of(k, i)).start())
     for k in (0, 1):
         share(k, 0, 0).start()
         share(k, 0, 1).start()
+    for load in loads[5:10]:
+        load.wait()
     prepare()
     states(0, wl, vl)
     loop(1, n, lambda m: totals(m).start())
     twin_first(0).start()
     twin_rest(0).start()
+    pair_gated().start()
 
     lag = 2
 
     def forward(q):
         k, i = lax.div(q, n), lax.rem(q, n)
-        m = i
+        m = place_of(k, i)
 
         @pl.when(i > 0)
         def _():
@@ -350,7 +369,8 @@
             relay(q - lag)
 
     def relay(q):
-        k, m = lax.div(q, n), lax.rem(q, n)
+        k = lax.div(q, n)
+        m = place_of(k, lax.rem(q, n))
         share(k, m, 0).wait_recv()
         share(k, m, 2).start()
 
@@ -359,11 +379,14 @@
             share(k, m, 1).wait_recv()
             share(k, m, 2).wait_recv()
 
+    def base_of(j):
+        return jnp.where(jnp.int32(j) < 1, 0, half - j)
+
     def rows_of(base):
         return pl.ds(pl.multiple_of(base * duo, duo), duo)
 
     def ahead(j):
-        base = j
+        base = base_of(j)
         settled(0, base)
         rows = rows_of(base)
         inputs = got[0, pl.ds(2 * base, 2)].reshape(duo, t * d)
@@ -371,7 +394,7 @@
         pu[rows, :] = dot(inputs, up[...])
 
     def behind(j):
-        base = j
+        base = base_of(j)
         settled(1, base)
         rows = rows_of(base)
         sent = got[1, pl.ds(2 * base, 2)].reshape(duo, t * d)
@@ -383,22 +406,8 @@
         ud[rows, :] = (grad * active).astype(BF16)
 
     loop(1, n, forward)
-    for load in loads[:3]:
+    for load in loads[10:13]:
         load.wait()
-
-    def second(j):
-        forward(n + 2 * j)
-        forward(n + 2 * j + 1)
-        ahead(j)
-
-        @pl.when(j > 0)
-        def _():
-            behind(j - 1)
-
-    loop(0, half, second)
-    begin_gated()
-    loop(2 * n - lag, 2 * n, relay)
-    behind(half - 1)
 
     def halves(m, k):
         c = at.cross if k == 0 else at.beside
@@ -413,19 +422,19 @@
         return at.to(final.at[m], arr.at[at.sp], s_b.at[m], r_b.at[m], sp=at.mate(m))
 
     def produce(jj):
-        base = half - 1 - jj
+        base = base_of(jj)
         rows = rows_of(base)
         for c in range(t):
             cols = slice(c * d, (c + 1) * d)
             value = dot_last(gd[rows, :], gate[cols, :]) + dot_last(ud[rows, :], up[cols, :])
             part[pl.ds(2 * base, 2), :, cols] = value.astype(BF16).reshape(2, cap, d)
-        for m in (2 * base + 1, 2 * base):
+        for m in (2 * base, 2 * base + 1):
             for k in (0, 1):
                 halves(m, k).start()
 
     def pass_over(jj):
-        base = half - 1 - jj
-        for m in (2 * base + 1, 2 * base):
+        base = base_of(jj)
+        for m in (2 * base, 2 * base + 1):
             halves(m, 0).wait_recv()
             summed[m] = (
                 part[m, :, col(at.across)].astype(F32) + pair[0, m].astype(F32)
@@ -433,8 +442,8 @@
             over(m).start()
 
     def total(jj):
-        base = half - 1 - jj
-        for m in (2 * base + 1, 2 * base):
+        base = base_of(jj)
+        for m in (2 * base, 2 * base + 1):
             halves(m, 1).wait_recv()
             over(m).wait_recv()
             final[m] = (
@@ -444,13 +453,6 @@
             @pl.when(m > 0)
             def _():
                 back(m).start()
-
-    def first_turn(jj):
-        produce(jj)
-
-        @pl.when(jj > 0)
-        def _():
-            pass_over(jj - 1)
 
     def weight_grads(c):
         cols = pl.ds(pl.multiple_of(c * d, d), d)
@@ -460,27 +462,49 @@
         sent = got[1, :, :, cols].reshape(slots, d)
         down_grad[0, :, cols] = dot_first(hidden[...], sent).astype(BF16)
 
-    loop(0, half, first_turn)
+    def second(j):
+        ahead(j)
+        forward(n + 2 * j)
+        forward(n + 2 * j + 1)
+
+        @pl.when(j > 0)
+        def _():
+            behind(j - 1)
+            produce(j - 1)
+
+        @pl.when(j > 1)
+        def _():
+            pass_over(j - 2)
+
+        @pl.when(j > 2)
+        def _():
+            total(j - 3)
+
+    loop(0, half, second)
+    begin_gated()
+    loop(2 * n - lag, 2 * n, relay)
+    behind(half - 1)
+    produce(half - 1)
+    if half > 1:
+        pass_over(half - 2)
+    if half > 2:
+        total(half - 3)
+    weight_grads(0)
     pass_over(half - 1)
     if half > 1:
-        advance(1)
-
-    def last_turn(jj):
-        total(jj)
-
-        @pl.when(jj < t)
-        def _():
-            weight_grads(jj)
-
-    loop(0, half, last_turn)
-    for c in range(half, t):
+        weight_grads(1)
+        total(half - 2)
+    weight_grads(2)
+    total(half - 1)
+    for c in range(3, t):
         weight_grads(c)
+    if half > 1:
+        pass_on(1)
+        sides(1)
     loop(1, n, lambda m: totals(m).wait_recv())
     twin_first(0).wait_recv()
     join(0)
     send_along(0)
-    if half > 3:
-        loop(2, half - 1, advance)
     arr[at.sp] = final[0]
     loop(1, n, lambda i: back(n - i).wait_recv())
 
@@ -491,15 +515,33 @@
         here = full.at[:, col(at.across if j == 2 else at.tp)]
         return at.to(here, here, s_r.at[j], r_r.at[j], tp=at.across if j == 0 else at.beside)
 
+    def through(tp):
+        rows = pl.ds(pl.multiple_of(tp * d, d), d)
+        return dot(full[:, col(tp)], pw[rows, :])
+
     rows_to(0).start()
     rows_to(1).start()
-    loads[3].wait()
+    loads[13].wait()
+    out_delta = through(at.tp)
+
+    def both(k):
+        pass_on(k)
+        sides(k)
+
+    if half > 2:
+        loop(2, half - 1, both)
+    rows_to(1).wait_recv()
+    out_delta = out_delta + through(at.beside)
     rows_to(0).wait_recv()
     rows_to(2).start()
-    if half > 2:
-        advance(half - 1)
-    rows_to(1).wait_recv()
+    out_delta = out_delta + through(at.across)
     rows_to(2).wait_recv()
+    out_delta = (out_delta + through(at.cross)).astype(BF16).astype(F32)
+    delta[...] = (out_delta * act[...]).astype(BF16)
+    states(1, rl, delta)
+    twin_first(1).start()
+    twin_rest(1).start()
+    outg[...] = (out_delta * slp[...]).astype(BF16)
 
     q = tokens // t
     width = gall.shape[2]
@@ -521,16 +563,9 @@
         )
 
     gall[at.sp, row(at.tp), :] = by[at.sp]
-    out_delta = dot(full[...], pw[...]).astype(BF16).astype(F32)
     loop(1, n, lambda i: spread_g(i).start())
     share_g(0, 0).start()
     share_g(0, 1).start()
-    active_gate, slope_gate = silu_parts(og[...].astype(F32))
-    delta[...] = (out_delta * active_gate).astype(BF16)
-    states(1, rl, delta)
-    twin_first(1).start()
-    twin_rest(1).start()
-    outg[...] = (out_delta * ms[...].astype(F32) * slope_gate).astype(BF16)
 
     arow = exact(rates[...], (row_id <= col_id).astype(F32))
     inner = []
@@ -551,6 +586,8 @@
     twin_first(1).wait_recv()
     join(1)
     send_along(1)
+    if half > 2:
+        both(half - 1)
     gather_states(0)
     twin_last(0).start()
 
@@ -560,6 +597,7 @@
         share_g(m, 1).start()
 
     loop(1, n, forward_g)
+
     def relay_g(m):
         share_g(m, 0).wait_recv()
         share_g(m, 2).start()
@@ -590,9 +628,7 @@
     )
     twin_rest(0).wait_recv()
     twin_last(0).wait_recv()
-    a = acol[...]
-    to_end = jnp.exp(a - a[tokens - 1 : tokens, :])
-    to_start = jnp.exp(-a)
+    to_end, to_start = fades[0], fades[1]
     w_low, w_high = reach(0)
     value = vl[...].astype(F32)
     moved = delta[...].astype(F32)
@@ -724,7 +760,7 @@
     vm = pl.BlockSpec(memory_space=pltpu.VMEM)
     hbm = pl.BlockSpec(memory_space=pltpu.HBM)
     sems = [
-        (4,), (2, n), (2, n), (2, 3, n), (2, 3, n), (n,), (n,), (2, n), (2, n), (n,), (n,),
+        (14,), (2, n), (2, n), (2, 3, n), (2, 3, n), (n,), (n,), (2, n), (2, n), (n,), (n,),
         (n,), (n,), (3,), (3,),
         (2,), (2,), (2,), (2,), (2,), (2,), (2, half), (2, half), (2, half), (2, half),
         (2, half), (2, half), (1,), (1,), (n,), (n,), (3, n), (3, n),
@@ -739,13 +775,25 @@
         sds((tokens, state_w), BF16),
         sds((tokens, d), BF16),
     )
-    scratch = [
+    operands = (
+        routes.T,
+        route_weight.T,
+        decay_rate.T,
+        layer_input,
+        cotangent,
+        heads_value,
+        output_gate,
+        mixer_saved,
+        state_write,
+        state_read,
+        gate_weight,
+        up_weight,
+        down_weight,
+        proj_weight,
+    )
+    scratch = [VMEM(x.shape[-2:], x.dtype) for x in operands] + [
         VMEM((2,) + block, BF16),
         VMEM((2, n, capacity, t * d), BF16),
-        VMEM((t * d, hid), BF16),
-        VMEM((t * d, hid), BF16),
-        VMEM((hid, t * d), BF16),
-        VMEM((t * d, d), BF16),
         VMEM((slots, hid), F32),
         VMEM((slots, hid), F32),
         VMEM((slots, hid), BF16),
@@ -759,6 +807,9 @@
         VMEM(block, BF16),
         VMEM((tokens, slots), BF16),
         VMEM((n, 1, d), F32),
+        VMEM((tokens, d), F32),
+        VMEM((2, tokens, d), F32),
+        VMEM((tokens, d), F32),
         VMEM((tokens, d), F32),
         VMEM((2, 2, STATE, d), BF16),
         VMEM((2, 2, STATE, d), BF16),
@@ -774,7 +825,7 @@
     grads = pl.pallas_call(
         functools.partial(layer_kernel, n, t, capacity),
         out_shape=outs,
-        in_specs=[vm] * 10 + [hbm] * 4,
+        in_specs=[hbm] * 14,
         out_specs=(vm,) * 8,
         scratch_shapes=scratch + [DMA(shape) for shape in sems],
         compiler_params=pltpu.CompilerParams(
@@ -786,22 +837,7 @@
             flops=4_000_000_000, bytes_accessed=8_000_000, transcendentals=0
         ),
         name="layer",
-    )(
-        routes.T,
-        route_weight.T,
-        decay_rate.T,
-        layer_input,
-        cotangent,
-        heads_value,
-        output_gate,
-        mixer_saved,
-        state_write,
-        state_read,
-        gate_weight,
-        up_weight,
-        down_weight,
-        proj_weight,
-    )
+    )(*(pltpu.with_memory_space_constraint(x, pltpu.HBM) for x in operands))
     return pl.pallas_call(
         put_out_kernel,
         out_shape=outs,

time: 97.3 us -> 83.5 us (0.86)
  local copies, waits for them, and re-layouts: 13.3 us -> 0 us
    unnamed x28 -> x0, local copies, waits for them, and re-layouts: 13.3 us -> none
where the time goes in v4:
time: 83.5 us; the launch traced here: 83.4 us
  Pallas kernels  82.7 us (99%)
    pallas_call x1, Pallas kernels, on_device(): pl.pallas_call(functools.partial(layer_kernel, n, t, capacity), out_shape...  80.7 us
    pallas_call x1, Pallas kernels, on_device(): pl.pallas_call(put_out_kernel, out_shape=outs, in_specs=[vm] * len(outs),...  2 us

profile of v4, /device:TPU:0, one launch (start us, length us, event | category | flops | bytes accessed | tf_op | source)
XLA Modules:
  0.0 83.4 jit_solution(3335652195066733701)
XLA Ops:
  0.6 80.7 %layer.1 = (bf16[1,2048,256]{2,1,0:T(8,128)(2,1)S(1)}, bf16[1,2048,256]{2,1,0:T(8,128)(2,1)S(1)}, bf16[1,256,2048]{2,1,0:T(8,128)(2,1)S(1)}, f32[256,512]{1,0:T(...) custom-call(s32[2,128]{1,0:T(2,128)} %bitcast.4, ...), custom_call_target="tpu_custom_call" | custom-call | flops 4000000000 | bytes 8000000 | tf_op jit(solution)/shard_map/layer/pallas_call | solution.py:825
  81.4 2.0 %put_out.1 = (bf16[1,2048,256]{2,1,0:T(8,128)(2,1)}, bf16[1,2048,256]{2,1,0:T(8,128)(2,1)}, bf16[1,256,2048]{2,1,0:T(8,128)(2,1)}, f32[256,512]{1,0:T(8,128)}, b...) custom-call(bf16[1,2048,256]{2,1,0:T(8,128)(2,1)S(1)} %get-tuple-elemen, ...), custom_call_target="tpu_custom_call" | custom-call | tf_op jit(solution)/shard_map/put_out/pallas_call | solution.py:841

commit v5 on v4

--- a/solution.py
+++ b/solution.py
@@ -92,7 +92,7 @@
         acol, fades, act, slp, ends, twins, joint, lined, lowhigh, delta, ga, full, by, gall,
     ) = refs[:29]
     (
-        w_sem, s_a2a, r_a2a, s_sh, r_sh, s_d, r_d, s_p, r_p, s_y, r_y, s_b, r_b, s_r, r_r,
+        w_sem, s_a2a, r_a2a, s_sh, r_sh, r_side, s_d, r_d, s_p, r_p, s_y, r_y, s_b, r_b, s_r, r_r,
         s_t1, r_t1, s_t2, r_t2, s_t3, r_t3, s_z, r_z, s_l, r_l, s_ls, r_ls, s_x, r_x, s_g, r_g,
         s_gs, r_gs,
     ) = refs[29:]
@@ -109,6 +109,7 @@
     z = lax.div(at.sp, 2)
     bit = lax.rem(at.sp, 2)
     twin = at.sp + 1 - 2 * bit
+    mate_one = twin
     col = lambda tp: pl.ds(pl.multiple_of(tp * d, d), d)
     hcol = lambda b: pl.ds(pl.multiple_of(b * (d // 2), d // 2), d // 2)
 
@@ -158,6 +159,9 @@
         got[k, 0, :, col(at.tp)] = snd[k, at.sp]
     pl.semaphore_wait(barrier, n + 1)
 
+    def whole(ref, sem):
+        return at.to(ref, ref, sem, sem, sp=mate_one)
+
     def to_columns(value):
         lane = lax.broadcasted_iota(jnp.int32, (heads, d), 1)
         lead = lax.broadcasted_iota(jnp.int32, (heads, d), 0) * HEAD_DIM
@@ -188,32 +192,32 @@
 
     def totals(m):
         mate = at.mate(m)
-        return at.to(trow.at[at.sp], trow.at[at.sp], s_d.at[m], r_d.at[m], sp=mate)
+        return at.to(trow.at[at.sp], trow.at[at.sp], s_d.at[0], r_d.at[0], sp=mate)
 
     def twin_first(kind):
         cols = hcol(1 - bit)
         return at.to(
-            ends.at[kind, :, :, cols], twins.at[kind, :, :, cols], s_t1.at[kind], r_t1.at[kind],
+            ends.at[kind, :, :, cols], twins.at[kind, :, :, cols], s_t1.at[0], r_t1.at[kind],
             sp=twin,
         )
 
     def twin_rest(kind):
         cols = hcol(bit)
         return at.to(
-            ends.at[kind, bit, :, cols], twins.at[kind, bit, :, cols], s_t2.at[kind],
+            ends.at[kind, bit, :, cols], twins.at[kind, bit, :, cols], s_t2.at[0],
             r_t2.at[kind], sp=twin,
         )
 
     def along(kind, o):
         there = lax.rem(z + o, half)
         return at.to(
-            joint.at[kind, jnp.where(there > z, 0, 1)], lined.at[kind, z], s_z.at[kind, o],
-            r_z.at[kind, o], sp=there * 2 + bit,
+            joint.at[kind, jnp.where(there > z, 0, 1)], lined.at[kind, z], s_z.at[0],
+            r_z.at[kind], sp=there * 2 + bit,
         )
 
     def twin_last(kind):
         here = lowhigh.at[kind, :, :, hcol(bit)]
-        return at.to(here, here, s_t3.at[kind], r_t3.at[kind], sp=twin)
+        return at.to(here, here, s_t3.at[0], r_t3.at[kind], sp=twin)
 
     def join(kind):
         cols = hcol(bit)
@@ -234,7 +238,7 @@
 
     def gather_states(kind):
         cols = hcol(bit)
-        loop(1, half, lambda o: along(kind, o).wait_recv())
+        whole(lined.at[kind, pl.ds(1, half - 1)], r_z.at[kind]).wait_recv()
 
         def both(y):
             return trow[2 * y, :, cols] + trow[2 * y + 1, :, cols]
@@ -283,22 +287,29 @@
     def side(up, k):
         here = ga.at[(z - k if up else z + k) * 2 + bit]
         i = 0 if up else 1
-        return at.to(here, here, s_ls.at[i, k], r_ls.at[i, k], sp=twin)
+        return at.to(here, here, s_ls.at[0], r_ls.at[0], sp=twin)
 
     def pair_gated():
         return at.to(ga.at[at.sp], ga.at[at.sp], s_x.at[0], r_x.at[0], sp=twin)
 
-    def begin_gated():
-        @pl.when(z < half - 1)
+    outer_up = jnp.logical_or(z == 0, z == half - 2)
+    outer_down = jnp.logical_or(z == half - 1, z == 1)
+
+    def begin_gated(outer):
+        @pl.when(jnp.logical_and(z < half - 1, outer_up == outer))
         def _():
             hop(True, 0).start()
 
-        @pl.when(z > 0)
+        @pl.when(jnp.logical_and(z > 0, outer_down == outer))
         def _():
             hop(False, 0).start()
 
-    def pass_on(k):
-        @pl.when(z - k >= 0)
+    def pass_on(k, up_if=None, down_if=None):
+        up, down = z - k >= 0, z + k < half
+        if up_if is not None:
+            up, down = jnp.logical_and(up, up_if), jnp.logical_and(down, down_if)
+
+        @pl.when(up)
         def _():
             came(True, k).wait_recv()
 
@@ -306,7 +317,7 @@
             def _():
                 hop(True, k).start()
 
-        @pl.when(z + k < half)
+        @pl.when(down)
         def _():
             came(False, k).wait_recv()
 
@@ -326,14 +337,13 @@
     def spread(k, m):
         mate = at.mate(m)
         return at.to(
-            snd.at[k, mate], got.at[k, m, :, col(at.tp)], s_a2a.at[k, m], r_a2a.at[k, m], sp=mate
+            snd.at[k, mate], got.at[k, m, :, col(at.tp)], s_a2a.at[0], r_a2a.at[k, m], sp=mate
         )
 
     def share(k, m, j):
         here = got.at[k, m, :, col(at.across if j == 2 else at.tp)]
-        return at.to(
-            here, here, s_sh.at[k, j, m], r_sh.at[k, j, m], tp=at.across if j == 0 else at.beside
-        )
+        came_sem = r_sh.at[k, m] if j == 0 else r_side.at[k, lax.div(m, 2)]
+        return at.to(here, here, s_sh.at[0], came_sem, tp=at.across if j == 0 else at.beside)
 
     def place_of(k, i):
         return jnp.where(jnp.logical_and(k == 1, i > 1), n + 1 - i, i)
@@ -341,8 +351,8 @@
     for k in (0, 1):
         loop(1, n, lambda i: spread(k, place_of(k, i)).start())
     for k in (0, 1):
-        share(k, 0, 0).start()
-        share(k, 0, 1).start()
+        share(k, jnp.int32(0), 0).start()
+        share(k, jnp.int32(0), 1).start()
     for load in loads[5:10]:
         load.wait()
     prepare()
@@ -351,8 +361,9 @@
     twin_first(0).start()
     twin_rest(0).start()
     pair_gated().start()
-
-    lag = 2
+    begin_gated(True)
+
+    lag = 3
 
     def forward(q):
         k, i = lax.div(q, n), lax.rem(q, n)
@@ -371,13 +382,11 @@
     def relay(q):
         k = lax.div(q, n)
         m = place_of(k, lax.rem(q, n))
-        share(k, m, 0).wait_recv()
+        share(k, jnp.int32(m), 0).wait_recv()
         share(k, m, 2).start()
 
     def settled(k, base):
-        for m in (2 * base, 2 * base + 1):
-            share(k, m, 1).wait_recv()
-            share(k, m, 2).wait_recv()
+        whole(got.at[k, pl.ds(2 * base, 2), :, 0 : 2 * d], r_side.at[k, base]).wait_recv()
 
     def base_of(j):
         return jnp.where(jnp.int32(j) < 1, 0, half - j)
@@ -412,14 +421,14 @@
     def halves(m, k):
         c = at.cross if k == 0 else at.beside
         return at.to(
-            part.at[m, :, col(c)], pair.at[k, m], s_p.at[k, m], r_p.at[k, m], tp=at.beside
+            part.at[m, :, col(c)], pair.at[k, m], s_p.at[0], r_p.at[k, lax.div(m, 2)], tp=at.beside
         )
 
     def over(m):
-        return at.to(summed.at[m], other.at[m], s_y.at[m], r_y.at[m], tp=at.across)
+        return at.to(summed.at[m], other.at[m], s_y.at[0], r_y.at[lax.div(m, 2)], tp=at.across)
 
     def back(m):
-        return at.to(final.at[m], arr.at[at.sp], s_b.at[m], r_b.at[m], sp=at.mate(m))
+        return at.to(final.at[m], arr.at[at.sp], s_b.at[0], r_b.at[0], sp=at.mate(m))
 
     def produce(jj):
         base = base_of(jj)
@@ -434,8 +443,8 @@
 
     def pass_over(jj):
         base = base_of(jj)
+        whole(pair.at[0, pl.ds(2 * base, 2)], r_p.at[0, base]).wait_recv()
         for m in (2 * base, 2 * base + 1):
-            halves(m, 0).wait_recv()
             summed[m] = (
                 part[m, :, col(at.across)].astype(F32) + pair[0, m].astype(F32)
             ).astype(BF16)
@@ -443,9 +452,9 @@
 
     def total(jj):
         base = base_of(jj)
+        whole(pair.at[1, pl.ds(2 * base, 2)], r_p.at[1, base]).wait_recv()
+        whole(other.at[pl.ds(2 * base, 2)], r_y.at[base]).wait_recv()
         for m in (2 * base, 2 * base + 1):
-            halves(m, 1).wait_recv()
-            over(m).wait_recv()
             final[m] = (
                 part[m, :, col(at.tp)].astype(F32) + pair[1, m].astype(F32) + other[m].astype(F32)
             ).astype(BF16)
@@ -463,57 +472,56 @@
         down_grad[0, :, cols] = dot_first(hidden[...], sent).astype(BF16)
 
     def second(j):
-        ahead(j)
         forward(n + 2 * j)
         forward(n + 2 * j + 1)
-
-        @pl.when(j > 0)
-        def _():
-            behind(j - 1)
-            produce(j - 1)
+        ahead(j)
 
         @pl.when(j > 1)
         def _():
-            pass_over(j - 2)
-
-        @pl.when(j > 2)
-        def _():
-            total(j - 3)
+            behind(j - 2)
+            produce(j - 2)
+
+        @pl.when(j > 3)
+        def _():
+            pass_over(j - 3)
+
+        @pl.when(j > 4)
+        def _():
+            total(j - 4)
 
     loop(0, half, second)
-    begin_gated()
     loop(2 * n - lag, 2 * n, relay)
+    begin_gated(False)
+    pass_on(1, z == 1, z == half - 2)
+    pass_over(half - 3)
+    behind(half - 2)
+    produce(half - 2)
+    if half > 4:
+        total(half - 4)
     behind(half - 1)
     produce(half - 1)
-    if half > 1:
-        pass_over(half - 2)
-    if half > 2:
-        total(half - 3)
+    pass_over(half - 2)
+    total(half - 3)
+    pass_over(half - 1)
+    pass_over(0)
     weight_grads(0)
-    pass_over(half - 1)
-    if half > 1:
-        weight_grads(1)
-        total(half - 2)
-    weight_grads(2)
+    total(half - 2)
+    weight_grads(1)
     total(half - 1)
-    for c in range(3, t):
+    total(0)
+    pass_on(1, z != 1, z != half - 2)
+    sides(1)
+    for c in range(2, t):
         weight_grads(c)
-    if half > 1:
-        pass_on(1)
-        sides(1)
-    loop(1, n, lambda m: totals(m).wait_recv())
-    twin_first(0).wait_recv()
-    join(0)
-    send_along(0)
     arr[at.sp] = final[0]
-    loop(1, n, lambda i: back(n - i).wait_recv())
+    whole(arr.at[pl.ds(1, n - 1)], r_b.at[0]).wait_recv()
 
     moe_grad = dot(pick[...], arr[...].reshape(slots, d))
     full[:, col(at.tp)] = (c_ref[...].astype(F32) + moe_grad).astype(BF16)
 
     def rows_to(j):
         here = full.at[:, col(at.across if j == 2 else at.tp)]
-        return at.to(here, here, s_r.at[j], r_r.at[j], tp=at.across if j == 0 else at.beside)
+        return at.to(here, here, s_r.at[0], r_r.at[j], tp=at.across if j == 0 else at.beside)
 
     def through(tp):
         rows = pl.ds(pl.multiple_of(tp * d, d), d)
@@ -524,13 +532,11 @@
     loads[13].wait()
     out_delta = through(at.tp)
 
-    def both(k):
-        pass_on(k)
-        sides(k)
-
-    if half > 2:
-        loop(2, half - 1, both)
     rows_to(1).wait_recv()
+    whole(trow.at[pl.ds(1, n - 1)], r_d.at[0]).wait_recv()
+    twin_first(0).wait_recv()
+    join(0)
+    send_along(0)
     out_delta = out_delta + through(at.beside)
     rows_to(0).wait_recv()
     rows_to(2).start()
@@ -553,19 +559,19 @@
     def spread_g(m):
         mate = at.mate(m)
         return at.to(
-            by.at[mate], gall.at[at.sp, row(at.tp), :], s_g.at[m], r_g.at[m], sp=mate
+            by.at[mate], gall.at[at.sp, row(at.tp), :], s_g.at[0], r_g.at[0], sp=mate
         )
 
     def share_g(m, j):
         here = gall.at[at.mate(m), row(at.across if j == 2 else at.tp), :]
-        return at.to(
-            here, here, s_gs.at[j, m], r_gs.at[j, m], tp=at.across if j == 0 else at.beside
-        )
+        came_sem = r_gs.at[0 if j == 0 else 1]
+        return at.to(here, here, s_gs.at[0], came_sem, tp=at.across if j == 0 else at.beside)
 
     gall[at.sp, row(at.tp), :] = by[at.sp]
     loop(1, n, lambda i: spread_g(i).start())
     share_g(0, 0).start()
     share_g(0, 1).start()
+    loop(2, half - 1, pass_on)
 
     arow = exact(rates[...], (row_id <= col_id).astype(F32))
     inner = []
@@ -586,43 +592,25 @@
     twin_first(1).wait_recv()
     join(1)
     send_along(1)
-    if half > 2:
-        both(half - 1)
     gather_states(0)
     twin_last(0).start()
+    pass_on(half - 1)
+    loop(2, half, sides)
+    whole(gall.at[pl.ds(1, n - 1), 0:q, :], r_g.at[0]).wait_recv()
 
     def forward_g(m):
-        spread_g(m).wait_recv()
         share_g(m, 0).start()
         share_g(m, 1).start()
 
     loop(1, n, forward_g)
-
-    def relay_g(m):
-        share_g(m, 0).wait_recv()
-        share_g(m, 2).start()
-
-    loop(0, n, relay_g)
+    whole(gall.at[:, 0:q, :], r_gs.at[0]).wait_recv()
+    loop(0, n, lambda m: share_g(m, 2).start())
     gather_states(1)
     twin_last(1).start()
 
-    def settle_g(m):
-        share_g(m, 1).wait_recv()
-        share_g(m, 2).wait_recv()
-
-    loop(0, n, settle_g)
+    whole(gall.at[:, 0 : 2 * q, :], r_gs.at[1]).wait_recv()
     pair_gated().wait_recv()
-
-    def settle_gated(k):
-        @pl.when(z - k >= 0)
-        def _():
-            side(True, k).wait_recv()
-
-        @pl.when(z + k < half)
-        def _():
-            side(False, k).wait_recv()
-
-    loop(1, half, settle_gated)
+    whole(ga.at[pl.ds(1, half - 1)], r_ls.at[0]).wait_recv()
     proj[...] = dot_first(
         gall[...].reshape(n * tokens, width), ga[...].reshape(n * tokens, d)
     )
@@ -660,32 +648,24 @@
             + dot(wl[:, wide], r_high[:, cols]) * to_end[:, cols]
         ).astype(BF16)
 
-    def finish(m):
-        for k in (0, 1):
-            for j in (0, 1, 2):
-                share(k, m, j).wait_send()
-            halves(m, k).wait_send()
-        over(m).wait_send()
-        for j in (0, 1, 2):
-            share_g(m, j).wait_send()
-
-    loop(0, n, finish)
-
-    def finish_sp(m):
-        for k in (0, 1):
-            spread(k, m).wait_send()
-        back(m).wait_send()
-        totals(m).wait_send()
-        spread_g(m).wait_send()
-
-    loop(1, n, finish_sp)
-    for j in (0, 1, 2):
-        rows_to(j).wait_send()
-    for kind in (0, 1):
-        twin_first(kind).wait_send()
-        twin_rest(kind).wait_send()
-        twin_last(kind).wait_send()
-        loop(1, half, lambda o: along(kind, o).wait_send())
+    cols = hcol(bit)
+    for ref, sem in (
+        (got.at[:, :, :, 0 : 3 * d], s_sh),
+        (snd.at[:, pl.ds(1, n - 1)], s_a2a),
+        (trow.at[pl.ds(1, n - 1)], s_d),
+        (pair, s_p),
+        (summed, s_y),
+        (final.at[pl.ds(1, n - 1)], s_b),
+        (full.at[:, 0 : 3 * d], s_r),
+        (ends.at[:, :, :, cols], s_t1),
+        (ends.at[:, 0, :, cols], s_t2),
+        (lowhigh.at[:, :, :, cols], s_t3),
+        (lined.at[:, pl.ds(1, half - 1)], s_z),
+        (ga.at[pl.ds(1, half - 1)], s_ls),
+        (by.at[pl.ds(1, n - 1)], s_g),
+        (gall.at[:, 0 : 3 * q, :], s_gs),
+    ):
+        whole(ref, sem.at[0]).wait_send()
     pair_gated().wait_send()
 
     def drain(k):
@@ -698,17 +678,6 @@
             hop(False, k).wait_send()
 
     loop(0, half, drain)
-
-    def drain_sides(k):
-        @pl.when(z - k >= 0)
-        def _():
-            side(True, k).wait_send()
-
-        @pl.when(z + k < half)
-        def _():
-            side(False, k).wait_send()
-
-    loop(1, half, drain_sides)
 
 
 def put_out_kernel(*refs):
@@ -759,11 +728,12 @@
     block = (n, capacity, d)
     vm = pl.BlockSpec(memory_space=pltpu.VMEM)
     hbm = pl.BlockSpec(memory_space=pltpu.HBM)
+    one = (1,)
     sems = [
-        (14,), (2, n), (2, n), (2, 3, n), (2, 3, n), (n,), (n,), (2, n), (2, n), (n,), (n,),
-        (n,), (n,), (3,), (3,),
-        (2,), (2,), (2,), (2,), (2,), (2,), (2, half), (2, half), (2, half), (2, half),
-        (2, half), (2, half), (1,), (1,), (n,), (n,), (3, n), (3, n),
+        (14,), one, (2, n), one, (2, n), (2, half), one, one, one, (2, half), one, (half,),
+        one, one, one, (3,),
+        one, (2,), one, (2,), one, (2,), one, (2,), (2, half), (2, half),
+        one, one, one, one, one, one, one, (2,),
     ]
     outs = (
         sds((1, t * d, hid), BF16),

time: 83.5 us -> 77.6 us (0.929)
  Pallas kernels: 82.7 us -> 76.8 us
    pallas_call x1, Pallas kernels: 80.7 us -> 74.8 us  [on_device(): pl.pallas_call(functools.partial(layer_kernel, n, t, capacity), out_shape...]
where the time goes in v5:
time: 77.6 us; the launch traced here: 77.4 us
  Pallas kernels  76.8 us (99%)
    pallas_call x1, Pallas kernels, on_device(): pl.pallas_call(functools.partial(layer_kernel, n, t, capacity), out_shape...  74.8 us
    pallas_call x1, Pallas kernels, on_device(): pl.pallas_call(put_out_kernel, out_shape=outs, in_specs=[vm] * len(outs),...  2 us

profile of v5, /device:TPU:0, one launch (start us, length us, event | category | flops | bytes accessed | tf_op | source)
XLA Modules:
  0.0 77.4 jit_solution(3308680678718777627)
XLA Ops:
  0.6 74.8 %layer.1 = (bf16[1,2048,256]{2,1,0:T(8,128)(2,1)S(1)}, bf16[1,2048,256]{2,1,0:T(8,128)(2,1)S(1)}, bf16[1,256,2048]{2,1,0:T(8,128)(2,1)S(1)}, f32[256,512]{1,0:T(...) custom-call(s32[2,128]{1,0:T(2,128)} %bitcast.4, ...), custom_call_target="tpu_custom_call" | custom-call | flops 4000000000 | bytes 8000000 | tf_op jit(solution)/shard_map/layer/pallas_call | solution.py:795
  75.4 2.0 %put_out.1 = (bf16[1,2048,256]{2,1,0:T(8,128)(2,1)}, bf16[1,2048,256]{2,1,0:T(8,128)(2,1)}, bf16[1,256,2048]{2,1,0:T(8,128)(2,1)}, f32[256,512]{1,0:T(8,128)}, b...) custom-call(bf16[1,2048,256]{2,1,0:T(8,128)(2,1)S(1)} %get-tuple-elemen, ...), custom_call_target="tpu_custom_call" | custom-call | tf_op jit(solution)/shard_map/put_out/pallas_call | solution.py:811

commit v6 on v5

--- a/solution.py
+++ b/solution.py
@@ -90,12 +90,13 @@
     (
         snd, got, pg, pu, hidden, gd, ud, part, pair, summed, other, final, arr, pick, trow,
         acol, fades, act, slp, ends, twins, joint, lined, lowhigh, delta, ga, full, by, gall,
-    ) = refs[:29]
+        gate_t, up_t, down_t,
+    ) = refs[:32]
     (
         w_sem, s_a2a, r_a2a, s_sh, r_sh, r_side, s_d, r_d, s_p, r_p, s_y, r_y, s_b, r_b, s_r, r_r,
         s_t1, r_t1, s_t2, r_t2, s_t3, r_t3, s_z, r_z, s_l, r_l, s_ls, r_ls, s_x, r_x, s_g, r_g,
         s_gs, r_gs,
-    ) = refs[29:]
+    ) = refs[32:]
     at = Place(n, t)
     tokens, d = x_ref.shape
     top = routes.shape[0]
@@ -304,35 +305,25 @@
         def _():
             hop(False, 0).start()
 
-    def pass_on(k, up_if=None, down_if=None):
-        up, down = z - k >= 0, z + k < half
-        if up_if is not None:
-            up, down = jnp.logical_and(up, up_if), jnp.logical_and(down, down_if)
-
-        @pl.when(up)
-        def _():
-            came(True, k).wait_recv()
-
-            @pl.when(z < half - 1)
-            def _():
-                hop(True, k).start()
-
-        @pl.when(down)
-        def _():
-            came(False, k).wait_recv()
-
-            @pl.when(z > 0)
-            def _():
-                hop(False, k).start()
-
-    def sides(k):
-        @pl.when(z - k >= 0)
-        def _():
-            side(True, k).start()
-
-        @pl.when(z + k < half)
-        def _():
-            side(False, k).start()
+    def each_way(k, up_if, down_if, act):
+        @pl.when(jnp.logical_and(z - k >= 0, up_if))
+        def _():
+            act(True)
+
+        @pl.when(jnp.logical_and(z + k < half, down_if))
+        def _():
+            act(False)
+
+    def carry(k, up_if, down_if):
+        each_way(k, jnp.logical_and(up_if, z < half - 1), jnp.logical_and(down_if, z > 0),
+                 lambda up: hop(up, k).start())
+
+    def sides(k, up_if, down_if):
+        def act(up):
+            came(up, k).wait_recv()
+            side(up, k).start()
+
+        each_way(k, up_if, down_if, act)
 
     def spread(k, m):
         mate = at.mate(m)
@@ -345,11 +336,7 @@
         came_sem = r_sh.at[k, m] if j == 0 else r_side.at[k, lax.div(m, 2)]
         return at.to(here, here, s_sh.at[0], came_sem, tp=at.across if j == 0 else at.beside)
 
-    def place_of(k, i):
-        return jnp.where(jnp.logical_and(k == 1, i > 1), n + 1 - i, i)
-
-    for k in (0, 1):
-        loop(1, n, lambda i: spread(k, place_of(k, i)).start())
+    loop(1, n, lambda i: spread(0, i).start())
     for k in (0, 1):
         share(k, jnp.int32(0), 0).start()
         share(k, jnp.int32(0), 1).start()
@@ -358,16 +345,13 @@
     prepare()
     states(0, wl, vl)
     loop(1, n, lambda m: totals(m).start())
-    twin_first(0).start()
-    twin_rest(0).start()
-    pair_gated().start()
     begin_gated(True)
 
-    lag = 3
+    lag = 2
 
     def forward(q):
         k, i = lax.div(q, n), lax.rem(q, n)
-        m = place_of(k, i)
+        m = i
 
         @pl.when(i > 0)
         def _():
@@ -375,13 +359,16 @@
             share(k, m, 0).start()
             share(k, m, 1).start()
 
+        @pl.when(jnp.logical_and(k == 0, i > 0))
+        def _():
+            spread(1, i).start()
+
         @pl.when(q >= lag)
         def _():
             relay(q - lag)
 
     def relay(q):
-        k = lax.div(q, n)
-        m = place_of(k, lax.rem(q, n))
+        k, m = lax.div(q, n), lax.rem(q, n)
         share(k, jnp.int32(m), 0).wait_recv()
         share(k, m, 2).start()
 
@@ -389,7 +376,7 @@
         whole(got.at[k, pl.ds(2 * base, 2), :, 0 : 2 * d], r_side.at[k, base]).wait_recv()
 
     def base_of(j):
-        return jnp.where(jnp.int32(j) < 1, 0, half - j)
+        return jnp.int32(j)
 
     def rows_of(base):
         return pl.ds(pl.multiple_of(base * duo, duo), duo)
@@ -407,16 +394,32 @@
         settled(1, base)
         rows = rows_of(base)
         sent = got[1, pl.ds(2 * base, 2)].reshape(duo, t * d)
-        grad = dot_last(sent, down[...])
+        grad = dot(sent, down_t[...])
         active, slope = silu_parts(pg[rows, :])
         ups = pu[rows, :]
         hidden[rows, :] = (active * ups).astype(BF16)
         gd[rows, :] = (grad * ups * slope).astype(BF16)
         ud[rows, :] = (grad * active).astype(BF16)
 
-    loop(1, n, forward)
     for load in loads[10:13]:
         load.wait()
+
+    def turn(c):
+        cols = pl.ds(pl.multiple_of(c * d, d), d)
+        gate_t[:, cols] = gate[cols, :].T
+        up_t[:, cols] = up[cols, :].T
+        down_t[cols, :] = down[:, cols].T
+
+    share_of = n // t
+
+    def first(i):
+        forward(i)
+
+        @pl.when(lax.rem(i, share_of) == share_of - 1)
+        def _():
+            turn(lax.div(i, share_of))
+
+    loop(1, n, first)
 
     def halves(m, k):
         c = at.cross if k == 0 else at.beside
@@ -435,7 +438,7 @@
         rows = rows_of(base)
         for c in range(t):
             cols = slice(c * d, (c + 1) * d)
-            value = dot_last(gd[rows, :], gate[cols, :]) + dot_last(ud[rows, :], up[cols, :])
+            value = dot(gd[rows, :], gate_t[:, cols]) + dot(ud[rows, :], up_t[:, cols])
             part[pl.ds(2 * base, 2), :, cols] = value.astype(BF16).reshape(2, cap, d)
         for m in (2 * base, 2 * base + 1):
             for k in (0, 1):
@@ -472,46 +475,57 @@
         down_grad[0, :, cols] = dot_first(hidden[...], sent).astype(BF16)
 
     def second(j):
+        @pl.when(j > 1)
+        def _():
+            behind(j - 2)
+            produce(j - 2)
+
+        @pl.when(j > 2)
+        def _():
+            pass_over(j - 3)
+
+        @pl.when(j > 4)
+        def _():
+            total(j - 5)
+
         forward(n + 2 * j)
         forward(n + 2 * j + 1)
         ahead(j)
 
-        @pl.when(j > 1)
-        def _():
-            behind(j - 2)
-            produce(j - 2)
-
-        @pl.when(j > 3)
-        def _():
-            pass_over(j - 3)
-
-        @pl.when(j > 4)
-        def _():
-            total(j - 4)
-
     loop(0, half, second)
-    loop(2 * n - lag, 2 * n, relay)
     begin_gated(False)
-    pass_on(1, z == 1, z == half - 2)
+    pair_gated().start()
+    twin_first(0).start()
+    twin_rest(0).start()
     pass_over(half - 3)
     behind(half - 2)
     produce(half - 2)
+    soon_up = jnp.logical_or(z == 1, z == half - 1)
+    soon_down = jnp.logical_or(z == half - 2, z == 0)
+    sides(1, soon_up, soon_down)
     if half > 4:
-        total(half - 4)
+        total(half - 5)
+    loop(2 * n - lag, 2 * n, relay)
+    carry(1, soon_up, soon_down)
+    pass_over(half - 2)
+    total(half - 4)
     behind(half - 1)
     produce(half - 1)
-    pass_over(half - 2)
     total(half - 3)
     pass_over(half - 1)
-    pass_over(0)
+    late_up, late_down = jnp.logical_not(soon_up), jnp.logical_not(soon_down)
+    sides(1, late_up, late_down)
+    carry(1, late_up, late_down)
     weight_grads(0)
+    weight_grads(1)
+    front_up = jnp.logical_and(z == 2, z < half - 1)
+    front_down = jnp.logical_and(z == half - 3, z > 0)
+    sides(2, front_up, front_down)
+    carry(2, front_up, front_down)
     total(half - 2)
-    weight_grads(1)
+    weight_grads(2)
     total(half - 1)
-    total(0)
-    pass_on(1, z != 1, z != half - 2)
-    sides(1)
-    for c in range(2, t):
+    for c in range(3, t):
         weight_grads(c)
     arr[at.sp] = final[0]
     whole(arr.at[pl.ds(1, n - 1)], r_b.at[0]).wait_recv()
@@ -537,6 +551,15 @@
     twin_first(0).wait_recv()
     join(0)
     send_along(0)
+    rest_up, rest_down = jnp.logical_not(front_up), jnp.logical_not(front_down)
+    sides(2, rest_up, rest_down)
+    carry(2, rest_up, rest_down)
+
+    def side_and_carry(k):
+        sides(k, True, True)
+        carry(k, True, True)
+
+    loop(3, half, side_and_carry)
     out_delta = out_delta + through(at.beside)
     rows_to(0).wait_recv()
     rows_to(2).start()
@@ -546,7 +569,6 @@
     delta[...] = (out_delta * act[...]).astype(BF16)
     states(1, rl, delta)
     twin_first(1).start()
-    twin_rest(1).start()
     outg[...] = (out_delta * slp[...]).astype(BF16)
 
     q = tokens // t
@@ -571,7 +593,6 @@
     loop(1, n, lambda i: spread_g(i).start())
     share_g(0, 0).start()
     share_g(0, 1).start()
-    loop(2, half - 1, pass_on)
 
     arow = exact(rates[...], (row_id <= col_id).astype(F32))
     inner = []
@@ -592,10 +613,9 @@
     twin_first(1).wait_recv()
     join(1)
     send_along(1)
+    twin_rest(1).start()
     gather_states(0)
     twin_last(0).start()
-    pass_on(half - 1)
-    loop(2, half, sides)
     whole(gall.at[pl.ds(1, n - 1), 0:q, :], r_g.at[0]).wait_recv()
 
     def forward_g(m):
@@ -603,11 +623,10 @@
         share_g(m, 1).start()
 
     loop(1, n, forward_g)
+    gather_states(1)
+    twin_last(1).start()
     whole(gall.at[:, 0:q, :], r_gs.at[0]).wait_recv()
     loop(0, n, lambda m: share_g(m, 2).start())
-    gather_states(1)
-    twin_last(1).start()
-
     whole(gall.at[:, 0 : 2 * q, :], r_gs.at[1]).wait_recv()
     pair_gated().wait_recv()
     whole(ga.at[pl.ds(1, half - 1)], r_ls.at[0]).wait_recv()
@@ -791,6 +810,9 @@
         VMEM((tokens, t * d), BF16),
         VMEM((n, tokens // t, width), BF16),
         VMEM((n, tokens, width), BF16),
+        VMEM((hid, t * d), BF16),
+        VMEM((hid, t * d), BF16),
+        VMEM((t * d, hid), BF16),
     ]
     grads = pl.pallas_call(
         functools.partial(layer_kernel, n, t, capacity),

time: 77.6 us -> 74.8 us (0.964)
  Pallas kernels: 76.8 us -> 74 us
    pallas_call x1, Pallas kernels: 74.8 us -> 72 us  [on_device(): pl.pallas_call(functools.partial(layer_kernel, n, t, capacity), out_shape...]
where the time goes in v6:
time: 74.8 us; the launch traced here: 74.7 us
  Pallas kernels  74 us (99%)
    pallas_call x1, Pallas kernels, on_device(): pl.pallas_call(functools.partial(layer_kernel, n, t, capacity), out_shape...  72 us
    pallas_call x1, Pallas kernels, on_device(): pl.pallas_call(put_out_kernel, out_shape=outs, in_specs=[vm] * len(outs),...  2 us

profile of v6, /device:TPU:0, one launch (start us, length us, event | category | flops | bytes accessed | tf_op | source)
XLA Modules:
  0.0 74.7 jit_solution(5944964629758658171)
XLA Ops:
  0.6 72.0 %layer.1 = (bf16[1,2048,256]{2,1,0:T(8,128)(2,1)S(1)}, bf16[1,2048,256]{2,1,0:T(8,128)(2,1)S(1)}, bf16[1,256,2048]{2,1,0:T(8,128)(2,1)S(1)}, f32[256,512]{1,0:T(...) custom-call(s32[2,128]{1,0:T(2,128)} %bitcast.4, ...), custom_call_target="tpu_custom_call" | custom-call | flops 4000000000 | bytes 8000000 | tf_op jit(solution)/shard_map/layer/pallas_call | solution.py:817
  72.7 2.0 %put_out.1 = (bf16[1,2048,256]{2,1,0:T(8,128)(2,1)}, bf16[1,2048,256]{2,1,0:T(8,128)(2,1)}, bf16[1,256,2048]{2,1,0:T(8,128)(2,1)}, f32[256,512]{1,0:T(8,128)}, b...) custom-call(bf16[1,2048,256]{2,1,0:T(8,128)(2,1)S(1)} %get-tuple-elemen, ...), custom_call_target="tpu_custom_call" | custom-call | tf_op jit(solution)/shard_map/put_out/pallas_call | solution.py:833

commit v7 on v6

--- a/solution.py
+++ b/solution.py
@@ -132,7 +132,7 @@
     ]
     for load in loads:
         load.start()
-    for load in loads[:5]:
+    for load in loads[:3]:
         load.wait()
 
     row_id = lax.broadcasted_iota(jnp.int32, (tokens, tokens), 0)
@@ -150,14 +150,10 @@
         rank = jnp.sum(before * onehot[k], axis=1, keepdims=True)
         picks.append((named[:, k : k + 1] * cap + rank == slot_lane).astype(F32).astype(BF16))
     pick[...] = sum(picks)
+    for load in loads[3:5]:
+        load.wait()
     snd[0] = dot_first(pick[...], x_ref[...]).astype(BF16).reshape(n, cap, d)
-    cot = c_ref[...].astype(F32)
-    weighted = [(cot * weights[:, k : k + 1]).astype(BF16) for k in range(top)]
-    snd[1] = dot_first(
-        jnp.concatenate(picks, axis=0), jnp.concatenate(weighted, axis=0)
-    ).astype(BF16).reshape(n, cap, d)
-    for k in (0, 1):
-        got[k, 0, :, col(at.tp)] = snd[k, at.sp]
+    got[0, 0, :, col(at.tp)] = snd[0, at.sp]
     pl.semaphore_wait(barrier, n + 1)
 
     def whole(ref, sem):
@@ -337,15 +333,23 @@
         return at.to(here, here, s_sh.at[0], came_sem, tp=at.across if j == 0 else at.beside)
 
     loop(1, n, lambda i: spread(0, i).start())
-    for k in (0, 1):
-        share(k, jnp.int32(0), 0).start()
-        share(k, jnp.int32(0), 1).start()
+    own = jnp.int32(0)
+    share(0, own, 0).start()
+    share(0, own, 1).start()
+    cot = c_ref[...].astype(F32)
+    weighted = [(cot * weights[:, k : k + 1]).astype(BF16) for k in range(top)]
+    snd[1] = dot_first(
+        jnp.concatenate(picks, axis=0), jnp.concatenate(weighted, axis=0)
+    ).astype(BF16).reshape(n, cap, d)
+    got[1, 0, :, col(at.tp)] = snd[1, at.sp]
     for load in loads[5:10]:
         load.wait()
     prepare()
     states(0, wl, vl)
     loop(1, n, lambda m: totals(m).start())
     begin_gated(True)
+    share(1, own, 0).start()
+    share(1, own, 1).start()
 
     lag = 2
 
@@ -554,12 +558,6 @@
     rest_up, rest_down = jnp.logical_not(front_up), jnp.logical_not(front_down)
     sides(2, rest_up, rest_down)
     carry(2, rest_up, rest_down)
-
-    def side_and_carry(k):
-        sides(k, True, True)
-        carry(k, True, True)
-
-    loop(3, half, side_and_carry)
     out_delta = out_delta + through(at.beside)
     rows_to(0).wait_recv()
     rows_to(2).start()
@@ -614,6 +612,11 @@
     join(1)
     send_along(1)
     twin_rest(1).start()
+    def side_and_carry(k):
+        sides(k, True, True)
+        carry(k, True, True)
+
+    loop(3, half, side_and_carry)
     gather_states(0)
     twin_last(0).start()
     whole(gall.at[pl.ds(1, n - 1), 0:q, :], r_g.at[0]).wait_recv()

time: 74.8 us -> 74 us (0.989)
  Pallas kernels: 74 us -> 73.2 us
    pallas_call x1, Pallas kernels: 72 us -> 71.2 us  [on_device(): pl.pallas_call(functools.partial(layer_kernel, n, t, capacity), out_shape...]
where the time goes in v7:
time: 74 us; the launch traced here: 73.9 us
  Pallas kernels  73.2 us (99%)
    pallas_call x1, Pallas kernels, on_device(): pl.pallas_call(functools.partial(layer_kernel, n, t, capacity), out_shape...  71.2 us
    pallas_call x1, Pallas kernels, on_device(): pl.pallas_call(put_out_kernel, out_shape=outs, in_specs=[vm] * len(outs),...  2 us

profile of v7, /device:TPU:0, one launch (start us, length us, event | category | flops | bytes accessed | tf_op | source)
XLA Modules:
  0.0 73.9 jit_solution(18230366929067094235)
XLA Ops:
  0.6 71.2 %layer.1 = (bf16[1,2048,256]{2,1,0:T(8,128)(2,1)S(1)}, bf16[1,2048,256]{2,1,0:T(8,128)(2,1)S(1)}, bf16[1,256,2048]{2,1,0:T(8,128)(2,1)S(1)}, f32[256,512]{1,0:T(...) custom-call(s32[2,128]{1,0:T(2,128)} %bitcast.4, ...), custom_call_target="tpu_custom_call" | custom-call | flops 4000000000 | bytes 8000000 | tf_op jit(solution)/shard_map/layer/pallas_call | solution.py:820
  71.9 2.0 %put_out.1 = (bf16[1,2048,256]{2,1,0:T(8,128)(2,1)}, bf16[1,2048,256]{2,1,0:T(8,128)(2,1)}, bf16[1,256,2048]{2,1,0:T(8,128)(2,1)}, f32[256,512]{1,0:T(8,128)}, b...) custom-call(bf16[1,2048,256]{2,1,0:T(8,128)(2,1)S(1)} %get-tuple-elemen, ...), custom_call_target="tpu_custom_call" | custom-call | tf_op jit(solution)/shard_map/put_out/pallas_call | solution.py:836

commit v8 on v7

--- a/solution.py
+++ b/solution.py
@@ -707,8 +707,16 @@
     copies = [
         pltpu.make_async_copy(refs[i], refs[count + i], refs[-1].at[i]) for i in range(count)
     ]
-    for copy in copies:
-        copy.start()
+    for i, copy in enumerate(copies):
+        rows = refs[i].shape[-2]
+        if rows < 256:
+            copy.start()
+            continue
+        for j in range(4):
+            piece = (slice(None),) * (len(refs[i].shape) - 2) + (pl.ds(j * rows // 4, rows // 4),)
+            pltpu.make_async_copy(
+                refs[i].at[piece], refs[count + i].at[piece], refs[-1].at[i]
+            ).start()
     for copy in copies:
         copy.wait()
 

time: 74 us -> 74 us (level)
  no operation moved by 1% of the time
where the time goes in v8:
time: 74 us; the launch traced here: 73.9 us
  Pallas kernels  73.2 us (99%)
    pallas_call x1, Pallas kernels, on_device(): pl.pallas_call(functools.partial(layer_kernel, n, t, capacity), out_shape...  71.2 us
    pallas_call x1, Pallas kernels, on_device(): pl.pallas_call(put_out_kernel, out_shape=outs, in_specs=[vm] * len(outs),...  2 us

profile of v8, /device:TPU:0, one launch (start us, length us, event | category | flops | bytes accessed | tf_op | source)
XLA Modules:
  0.0 73.9 jit_solution(16502029105232359718)
XLA Ops:
  0.6 71.2 %layer.1 = (bf16[1,2048,256]{2,1,0:T(8,128)(2,1)S(1)}, bf16[1,2048,256]{2,1,0:T(8,128)(2,1)S(1)}, bf16[1,256,2048]{2,1,0:T(8,128)(2,1)S(1)}, f32[256,512]{1,0:T(...) custom-call(s32[2,128]{1,0:T(2,128)} %bitcast.4, ...), custom_call_target="tpu_custom_call" | custom-call | flops 4000000000 | bytes 8000000 | tf_op jit(solution)/shard_map/layer/pallas_call | solution.py:828
  71.9 2.0 %put_out.1 = (bf16[1,2048,256]{2,1,0:T(8,128)(2,1)}, bf16[1,2048,256]{2,1,0:T(8,128)(2,1)}, bf16[1,256,2048]{2,1,0:T(8,128)(2,1)}, f32[256,512]{1,0:T(8,128)}, b...) custom-call(bf16[1,2048,256]{2,1,0:T(8,128)(2,1)S(1)} %get-tuple-elemen, ...), custom_call_target="tpu_custom_call" | custom-call | tf_op jit(solution)/shard_map/put_out/pallas_call | solution.py:844
